TPU v7x, 32 devices: a whole 2x2x4 slice. The times are simulated.
32 devices in a mesh: sp: 8 (over z, y), tp: 4 (over x, core).
Axes of the slice: x: 2, y: 2, z: 4, core: 2. Of those that a mesh axis runs over, the one named last changes fastest.
Arguments:
- tokens: bfloat16 [8192, 4096], P('sp', 'tp'), may hold values from -6 to 6
- norm_gain: float32 [4096], replicated, may hold values from 0.1 to 1.9
- pool_in_weight: bfloat16 [4096, 2048], P('sp', 'tp'), may hold values from -0.09375 to 0.09375
- query_weight: bfloat16 [4096, 2048], P('sp', 'tp'), may hold values from -1 to 1, as said below
- key_weight: bfloat16 [4096, 512], P('sp', 'tp'), may hold values from -40 to 40
- value_weight: bfloat16 [4096, 512], P('sp', 'tp'), may hold values from -0.09375 to 0.09375
- pool_weight: bfloat16 [8, 256, 256], P('tp'), may hold values from -0.375 to 0.375
- pool_scale: float32 [2048], P('tp'), may hold values from 0.1 to 1.9
- sink_logit: float32 [32], P('tp'), may hold values from 3 to 7
- out_pool_weight: bfloat16 [2048, 4096], P('tp', 'sp'), may hold values from -0.09375 to 0.09375
- out_attn_weight: bfloat16 [2048, 4096], P('tp', 'sp'), may hold values from -1.5 to 1.5
Outputs:
- mixed: bfloat16 [8192, 4096], P(('sp', 'tp'))
Inputs may be any that keep to these rules, and one draw needn't show every extreme that they name: `query_weight`: entries of order 4096 ** -0.5, drawn independently.
All inputs are finite; a program needn't handle non-finite values.
Results may differ from a plain program's by a relative error of at most 0.014.
The roundings to bfloat16 on the way count: a program that leaves them out, or rounds other values in their place, can miss the bound.
Values may be sent and summed in bfloat16 or wider, within the bound.
A program may use at most 128 MiB of HBM per device.

v0:
```python
import jax
import jax.numpy as jnp
from jax import lax
from jax.sharding import PartitionSpec as P

HEAD_DIM = 64
Q_HEADS = 32
KV_HEADS = 8
GROUP_DIM = 256
WINDOW = 128
GRID_W = 64


epsilon = 1e-06
rotary_base = 10000.0
masked_score = -1e30


def padded(block, sides, width):
    for axis, dim in sides:
        count = lax.axis_size(axis)
        forward = [(i, i + 1) for i in range(count - 1)]
        backward = [(target, source) for source, target in forward]
        low = lax.ppermute(
            lax.slice_in_dim(block, block.shape[dim] - width, None, axis=dim), axis, forward
        )
        high = lax.ppermute(lax.slice_in_dim(block, 0, width, axis=dim), axis, backward)
        block = jnp.concatenate([low, block, high], axis=dim)
    return block


def rms_normed(values, gain):
    floats = values.astype(jnp.float32)
    scaled = floats * lax.rsqrt(jnp.mean(floats * floats, axis=-1, keepdims=True) + epsilon)
    return (scaled * gain).astype(jnp.bfloat16)


def rotary_tables(positions, head_dim, grid_width):
    freq_count = head_dim // 4
    inverse = rotary_base ** (-jnp.arange(freq_count, dtype=jnp.float32) / freq_count)
    row_pos = (positions // grid_width).astype(jnp.float32)
    col_pos = (positions % grid_width).astype(jnp.float32)
    angles = jnp.stack([row_pos[:, None] * inverse, col_pos[:, None] * inverse], axis=1)
    return (jnp.cos(angles), jnp.sin(angles))


def rotate(values, cosine, sine):
    length, heads, head_dim = values.shape
    split = values.reshape(length, heads, 2, 2, head_dim // 4)
    first = split[:, :, :, 0]
    second = split[:, :, :, 1]
    cos_b = cosine[:, None]
    sin_b = sine[:, None]
    turned = jnp.stack([first * cos_b - second * sin_b, second * cos_b + first * sin_b], axis=3)
    return turned.reshape(length, heads, head_dim)


def rows_over_tp(tokens):
    count = lax.axis_size("tp")
    me = lax.axis_index("tp")
    rows, width = tokens.shape
    whole = jnp.zeros((rows, width * count), tokens.dtype)
    held = [(me, tokens)]
    for step in range(2, count, 2):
        moved = lax.ppermute(tokens, "tp", [(i, (i + step) % count) for i in range(count)])
        held.append(((me - step) % count, moved))
    swap = [(i, i ^ 1) for i in range(count)]
    held += [(owner ^ 1, lax.ppermute(piece, "tp", swap)) for owner, piece in held]
    for owner, piece in held:
        whole = lax.dynamic_update_slice_in_dim(whole, piece, owner * width, 1)
    return whole


def ring_gather(block, dim):
    count = lax.axis_size("sp")
    order = list(range(0, count, 2)) + list(range(count - 1, 0, -2))
    ahead = [(order[i], order[(i + 1) % count]) for i in range(count)]
    back = [(b, a) for a, b in ahead]
    me = lax.axis_index("sp")
    place = jnp.where(me % 2 == 0, me // 2, count - 1 - me // 2)
    split = 1 - dim
    size = block.shape[split] // 2
    width = block.shape[dim]
    shape = list(block.shape)
    shape[dim] *= count
    whole = jnp.zeros(shape, block.dtype)
    whole = lax.dynamic_update_slice_in_dim(whole, block, me * width, dim)
    for half, perm, sign in ((0, ahead, -1), (1, back, 1)):
        piece = lax.slice_in_dim(block, half * size, (half + 1) * size, axis=split)
        for step in range(1, count):
            piece = lax.ppermute(piece, "sp", perm)
            spot = (place + sign * step) % count
            owner = jnp.where(spot < count // 2, 2 * spot, 2 * (count - 1 - spot) + 1)
            starts = [half * size, half * size]
            starts[dim] = owner * width
            whole = lax.dynamic_update_slice(whole, piece, starts)
    return whole


def summed_over_tp(mixers, weight):
    count = lax.axis_size("tp")
    me = lax.axis_index("tp")
    rows = mixers.shape[0] // count
    swap = [(i, i ^ 1) for i in range(count)]

    def partial(owner):
        piece = lax.dynamic_slice_in_dim(mixers, owner * rows, rows, 0)
        return jnp.dot(piece, weight, preferred_element_type=jnp.float32).astype(jnp.bfloat16)

    total = None
    arrived = []
    for step in list(range(2, count, 2)) + [0]:
        owner = (me + step) % count
        other = lax.ppermute(partial(owner ^ 1), "tp", swap)
        both = partial(owner).astype(jnp.float32) + other.astype(jnp.float32)
        if step:
            perm = [(i, (i + step) % count) for i in range(count)]
            arrived.append(lax.ppermute(both.astype(jnp.bfloat16), "tp", perm))
        else:
            total = both
    for piece in arrived:
        total = total + piece.astype(jnp.float32)
    return total.astype(jnp.bfloat16)


def shards(
    tokens,
    norm_gain,
    pool_in_weight,
    query_weight,
    key_weight,
    value_weight,
    pool_weight,
    pool_scale,
    sink_logit,
    out_pool_weight,
    out_attn_weight,
):
    in_weight = jnp.concatenate([pool_in_weight, query_weight, key_weight, value_weight], axis=1)
    in_full = lax.all_gather(in_weight, "sp", axis=0, tiled=True)
    whole_rows = rows_over_tp(tokens)
    normed = rms_normed(whole_rows, norm_gain)
    tok_rows = normed.shape[0]
    raw = jnp.dot(normed, in_full, preferred_element_type=jnp.float32)
    ends = [pool_in_weight.shape[1], query_weight.shape[1], key_weight.shape[1]]
    pool_raw, query_raw, key_raw, value_raw = jnp.split(
        raw, [ends[0], ends[0] + ends[1], sum(ends)], axis=1
    )
    sp_index = lax.axis_index("sp")
    tp_index = lax.axis_index("tp")
    total_rows = tok_rows * lax.axis_size("sp")
    offset = sp_index * tok_rows
    positions = offset + jnp.arange(tok_rows, dtype=jnp.int32)
    cosine, sine = rotary_tables(positions, HEAD_DIM, GRID_W)
    pool_in = pool_raw.astype(jnp.bfloat16)
    queries = rotate(query_raw.reshape(tok_rows, -1, HEAD_DIM), cosine, sine).astype(jnp.bfloat16)
    key_part = rotate(key_raw.reshape(tok_rows, -1, HEAD_DIM), cosine, sine).astype(jnp.bfloat16)
    key_part = key_part.reshape(tok_rows, -1)
    value_part = value_raw.astype(jnp.bfloat16)
    kv_rows = jnp.concatenate([key_part, value_part], axis=1)
    kv_width = key_part.shape[1]
    channels = pool_in.shape[1]
    pool_reach = 8
    pool_pad = padded(pool_in, (("sp", 0),), pool_reach)
    kv_pad = padded(kv_rows, (("sp", 0),), WINDOW)
    running = jnp.concatenate(
        [jnp.zeros((1, channels), jnp.float32), jnp.cumsum(pool_pad.astype(jnp.float32), axis=0)],
        axis=0,
    )
    groups_dev = channels // GROUP_DIM
    selector = (tp_index * groups_dev + jnp.arange(channels, dtype=jnp.int32) // GROUP_DIM) % 4
    window_mean = jnp.zeros((tok_rows, channels), jnp.float32)
    for level, half_width in enumerate((1, 2, 4, 8)):
        window_sum = (
            running[pool_reach + half_width : pool_reach + half_width + tok_rows]
            - running[pool_reach - half_width : pool_reach - half_width + tok_rows]
        )
        counts = jnp.minimum(positions + half_width, total_rows) - jnp.maximum(
            positions - half_width, 0
        )
        level_mean = window_sum / counts.astype(jnp.float32)[:, None]
        window_mean = jnp.where((selector == level)[None, :], level_mean, window_mean)
    pooled = (window_mean - pool_in.astype(jnp.float32)).astype(jnp.bfloat16)
    mixing = jnp.einsum(
        "tgc,gcd->tgd",
        pooled.reshape(tok_rows, groups_dev, GROUP_DIM),
        pool_weight,
        preferred_element_type=jnp.float32,
    )
    pool_out = (mixing.reshape(tok_rows, channels) * pool_scale).astype(jnp.bfloat16)
    group = Q_HEADS // KV_HEADS
    kv_heads_dev = kv_width // HEAD_DIM
    query_groups = queries.reshape(tok_rows, kv_heads_dev, group, HEAD_DIM)
    key_pad = kv_pad[:, :kv_width].reshape(-1, kv_heads_dev, HEAD_DIM)
    value_pad = kv_pad[:, kv_width:].reshape(-1, kv_heads_dev, HEAD_DIM)
    block = 2 * WINDOW
    blocks = tok_rows // block
    span = block + 2 * WINDOW
    query_groups = query_groups.reshape(blocks, block, kv_heads_dev, group, HEAD_DIM)

    def windows(padded_rows):
        return jnp.stack([padded_rows[i * block : i * block + span] for i in range(blocks)])

    scores = jnp.einsum(
        "bqkgd,bskd->bkgqs", query_groups, windows(key_pad), preferred_element_type=jnp.float32
    ) * HEAD_DIM ** (-0.5)
    query_pos = positions.reshape(blocks, block)
    key_pos = query_pos[:, :1] - WINDOW + jnp.arange(span, dtype=jnp.int32)
    allowed = (
        (jnp.abs(key_pos[:, None, :] - query_pos[:, :, None]) <= WINDOW)
        & (key_pos >= 0)[:, None, :]
        & (key_pos < total_rows)[:, None, :]
    )
    scores = jnp.where(allowed[:, None, None], scores, masked_score)
    sink = sink_logit.reshape(1, kv_heads_dev, group, 1, 1)
    highest = jnp.maximum(jnp.max(scores, axis=-1, keepdims=True), sink)
    expo = jnp.exp(scores - highest)
    denominator = jnp.sum(expo, axis=-1, keepdims=True) + jnp.exp(sink - highest)
    weights = (expo / denominator).astype(jnp.bfloat16)
    attended = jnp.einsum(
        "bkgqs,bskd->bqkgd", weights, windows(value_pad), preferred_element_type=jnp.float32
    )
    attn_out = attended.reshape(tok_rows, -1).astype(jnp.bfloat16)
    out_weight = jnp.concatenate([out_pool_weight, out_attn_weight], axis=0)
    out_full = ring_gather(out_weight, 1)
    mixers = jnp.concatenate([pool_out, attn_out], axis=1)
    return summed_over_tp(mixers, out_full)


def solution(mesh):
    return jax.shard_map(
        shards,
        mesh=mesh,
        in_specs=(
            P("sp", "tp"),
            P(),
            P("sp", "tp"),
            P("sp", "tp"),
            P("sp", "tp"),
            P("sp", "tp"),
            P("tp", None, None),
            P("tp"),
            P("tp"),
            P("tp", "sp"),
            P("tp", "sp"),
        ),
        out_specs=P(("sp", "tp"), None),
        check_vma=False,
    )
```

profile of v0, /device:TPU:4, one launch (start us, length us, event | category | flops | bytes accessed | tf_op | source)
XLA Modules:
  0.0 414.1 jit_solution(16091095112114541333)
XLA Ops:
  12.7 11.0 %collective-permute-done.7 = bf16[512,512]{1,0:T(8,128)(2,1)S(1)} collective-permute-done((bf16[512,512]{1,0:T(8,128)(2,1)}, bf16[512,512]{1,0:T(8,128)(2,1)S(1)}, u32[]{:S(2)}, u32[]{:S(2)}) %collective-permute-start.7) | collective-permute-done | bytes 524320 | tf_op jit(solution)/shard_map/ppermute | solution.py:91
  26.5 4.0 collective-permute-start.15
  30.6 31.8 %collective-permute-done.8 = bf16[512,512]{1,0:T(8,128)(2,1)S(1)} collective-permute-done((bf16[512,512]{1,0:T(8,128)(2,1)S(1)}, bf16[512,512]{1,0:T(8,128)(2,1)S(1)}, u32[]{:S(2)}, u32[]{:S(2)}) %collective-permute-start.8) | collective-permute-done | bytes 524320 | tf_op jit(solution)/shard_map/ppermute | solution.py:91
  64.3 3.2 collective-permute-start.16
  68.1 19.7 %collective-permute-done.9 = bf16[512,512]{1,0:T(8,128)(2,1)} collective-permute-done((bf16[512,512]{1,0:T(8,128)(2,1)S(1)}, bf16[512,512]{1,0:T(8,128)(2,1)}, u32[]{:S(2)}, u32[]{:S(2)}) %collective-permute-start.9) | collective-permute-done | bytes 524320 | tf_op jit(solution)/shard_map/ppermute | solution.py:91
  91.9 19.7 %collective-permute-done.10 = bf16[512,512]{1,0:T(8,128)(2,1)} collective-permute-done((bf16[512,512]{1,0:T(8,128)(2,1)}, bf16[512,512]{1,0:T(8,128)(2,1)}, u32[]{:S(2)}, u32[]{:S(2)}) %collective-permute-start.10) | collective-permute-done | bytes 524320 | tf_op jit(solution)/shard_map/ppermute | solution.py:91
  114.9 8.4 %collective-permute-start.18 = (bf16[512,512]{1,0:T(8,128)(2,1)}, bf16[512,512]{1,0:T(8,128)(2,1)}, u32[]{:S(2)}, u32[]{:S(2)}) collective-permute-start(bf16[512,512]{1,0:T(8,128)(2,1)} %collective-permute-done.17), channel_id=1, source_target_pairs={{8,0},{16,8},{24,16},{28,24},{20,28},{12,20},{4,12},{0,4},{9,1},{1... | collective-permute-start | bytes 1572872 | tf_op jit(solution)/shard_map/ppermute | solution.py:91
  123.3 4.5 %broadcast.572.clone = bf16[1024,4096]{1,0:T(8,128)(2,1)} broadcast(bf16[]{:T(256)} %constant.217.clone.1), dimensions={} | broadcast | bytes 8388610 | tf_op jit(solution)/shard_map/broadcast.23
  129.0 25.3 %collective-permute-done.11 = bf16[512,512]{1,0:T(8,128)(2,1)} collective-permute-done((bf16[512,512]{1,0:T(8,128)(2,1)}, bf16[512,512]{1,0:T(8,128)(2,1)}, u32[]{:S(2)}, u32[]{:S(2)}) %collective-permute-start.11) | collective-permute-done | bytes 524320 | tf_op jit(solution)/shard_map/ppermute | solution.py:91
  165.2 30.0 %collective-permute-done.12 = bf16[512,512]{1,0:T(8,128)(2,1)S(1)} collective-permute-done((bf16[512,512]{1,0:T(8,128)(2,1)}, bf16[512,512]{1,0:T(8,128)(2,1)S(1)}, u32[]{:S(2)}, u32[]{:S(2)}) %collective-permute-start.12) | collective-permute-done | bytes 524320 | tf_op jit(solution)/shard_map/ppermute | solution.py:91
  197.1 3.1 constant_dynamic-update-slice_fusion.8
  205.2 14.2 %collective-permute-done.13 = bf16[512,512]{1,0:T(8,128)(2,1)S(1)} collective-permute-done((bf16[512,512]{1,0:T(8,128)(2,1)S(1)}, bf16[512,512]{1,0:T(8,128)(2,1)S(1)}, u32[]{:S(2)}, u32[]{:S(2)}) %collective-permute-start.13) | collective-permute-done | bytes 524320 | tf_op jit(solution)/shard_map/ppermute | solution.py:91
  233.1 17.8 %fusion.93 = (bf16[1024,1280]{1,0:T(8,128)(2,1)}, f32[1024,1280]{1,0:T(8,128)S(1)}) fusion(bf16[4096,1280]{1,0:T(8,128)(2,1)} %all-gather.2.cloned.1.call-done, bf16[1024,4096]{1,0:T(8,128)(2,1)} %copy-done.4, f32[4096]{0:T(1024)S(1)} %copy-done.30, f32[1024]{0:T(1024)S(1)} %add_rsqrt_fusion), kind=kOutput, calls=%fused_computation.186 | convolution fusion | flops 10755506176 | bytes 26759168 | tf_op jit(solution)/shard_map/dot_general | solution.py:144
  265.1 4.5 %collective-permute-start.6 = (bf16[128,256]{1,0:T(8,128)(2,1)}, bf16[128,256]{1,0:T(8,128)(2,1)}, u32[]{:S(2)}, u32[]{:S(2)}) collective-permute-start(bf16[128,256]{1,0:T(8,128)(2,1)} %get-tuple-element.20), channel_id=1, source_target_pairs={{4,0},{8,4},{12,8},{16,12},{20,16},{24,20},{28,24},{5,1},{9,5},{13... | collective-permute-start | bytes 196616 | tf_op jit(solution)/shard_map/ppermute | solution.py:27
  276.1 3.4 collective-permute-start.4
  293.8 4.2 %fusion.32 = bf16[1024,512]{1,0:T(8,128)(2,1)S(1)} fusion(f32[1152,512]{1,0:T(8,128)S(1)} %bitcast.74, f32[1040,512]{1,0:T(8,128)S(1)} %slice.160, f32[1024]{0:T(1024)S(1)} %get-tuple-element.35, f32[1024]{0:T(1024)S(1)} %copy-done.20, f32[1024]{0:T(1024)S(1)} %copy-done.21, f32[1024]{0:T(1024)S(1)} %copy-done.22, pred[512]{0:T(512)(128)(4,1)S(1)} %copy-done.28, ...), kind=kLoop, calls=%fused_computation.55 | loop fusion | flops 7864320 | bytes 18925568 | tf_op jit(solution)/shard_map/convert_element_type | solution.py:183
  300.2 7.4 %fusion.4 = (f32[4,2,4,256]{3,2,1,0:T(4,128)S(1)}, f32[4,2,512,256,4]{3,2,4,1,0:T(8,128)}) fusion(pred[4,256,512]{1,2,0:T(8,128)(4,1)S(1)} %copy-done.8, bf16[4,256,2,4,64]{1,0,4,3,2:T(4,128)(2,1)S(1)} %copy-done.10, bf16[1,512,2,64]{1,3,2,0:T(8,128)(2,1)S(1)} %bitcast.90, bf16[1,512,2,64]{1,3,2,0:T(8,128)(2,1)S(1)} %bitcast.93, ...), kind=kOutput, calls=%fused_computation.9 | convolution fusion | flops 551542784 | bytes 18907136 | tf_op jit(solution)/shard_map/bqkgd,bskd->bkgqs/dot_general | solution.py:204
  307.7 9.5 %fusion.3 = f32[4,2,4,256]{3,2,1,0:T(4,128)S(1)} fusion(f32[4,2,512,256,4]{3,2,4,1,0:T(8,128)} %get-tuple-element.32, f32[4,2,4,256]{3,2,1,0:T(4,128)S(1)} %broadcast_maximum_fusion, pred[4,256,512]{1,2,0:T(8,128)(4,1)S(1)} %copy-done.8), kind=kLoop, calls=%fused_computation.8 | loop fusion | flops 16769024 | bytes 17367040 | tf_op jit(solution)/shard_map/reduce_sum | solution.py:218
  317.5 8.5 %fusion.34 = bf16[4,256,2,4,64]{1,4,3,2,0:T(8,128)(2,1)S(1)} fusion(f32[4,2,512,256,4]{3,2,4,1,0:T(8,128)} %get-tuple-element.32, f32[4,2,4,256]{3,2,1,0:T(4,128)S(1)} %exponential_add_fusion, f32[4,2,4,256]{3,2,1,0:T(4,128)S(1)} %broadcast_maximum_fusion, pred[4,256,512]{1,2,0:T(8,128)(4,1)S(1)} %copy-done.8, bf16[1,512,2,64]{1,3,2,0:T(8,128)(2,1)S(1)} %bitcast.91, ...), kind=kOutput, calls=%fused_computation.57 | convolution fusion | flops 560463872 | bytes 18939904 | tf_op jit(solution)/shard_map/bkgqs,bskd->bqkgd/dot_general | solution.py:220
  327.1 7.2 %convolution_convert_fusion = bf16[256,4096]{1,0:T(8,128)(2,1)} fusion(bf16[1024,4096]{1,0:T(8,128)(2,1)} %constant_dynamic-update-slice_fusion.11, s32[]{:T(128)S(6)} %select_n.332, bf16[1024,512]{0,1:T(8,128)(2,1)S(1)} %fusion.29, bf16[1024,512]{0,1:T(8,128)(2,1)S(1)} %bitcast.75), kind=kOutput, calls=%fused_computation.14 | convolution fusion | flops 2149580800 | bytes 12582916 | tf_op jit(solution)/shard_map/dot_general | solution.py:108
  334.3 7.2 %convolution_convert_fusion.2 = bf16[256,4096]{1,0:T(8,128)(2,1)} fusion(bf16[1024,4096]{1,0:T(8,128)(2,1)} %constant_dynamic-update-slice_fusion.11, s32[]{:T(128)S(6)} %select_n.329, bf16[1024,512]{0,1:T(8,128)(2,1)S(1)} %fusion.29, bf16[1024,512]{0,1:T(8,128)(2,1)S(1)} %bitcast.76), kind=kOutput, calls=%fused_computation.18 | convolution fusion | flops 2149580800 | bytes 12582916 | tf_op jit(solution)/shard_map/dot_general | solution.py:108
  342.0 8.0 %fusion.16 = bf16[256,4096]{1,0:T(8,128)(2,1)} fusion(bf16[1024,4096]{1,0:T(8,128)(2,1)} %constant_dynamic-update-slice_fusion.11, bf16[256,4096]{1,0:T(8,128)(2,1)} %collective-permute-done.22, s32[]{:T(128)S(6)} %select_n.331, bf16[1024,512]{0,1:T(8,128)(2,1)S(1)} %fusion.29, bf16[1024,512]{0,1:T(8,128)(2,1)S(1)} %bitcast.77), kind=kOutput, calls=%fused_computation.24 | convolution fusion | flops 2153775104 | bytes 14680068 | tf_op jit(solution)/shard_map/dot_general | solution.py:108
  351.6 46.3 %collective-permute-done.23 = bf16[256,4096]{1,0:T(8,128)(2,1)} collective-permute-done((bf16[256,4096]{1,0:T(8,128)(2,1)}, bf16[256,4096]{1,0:T(8,128)(2,1)}, u32[]{:S(2)}, u32[]{:S(2)}) %collective-permute-start.23) | collective-permute-done | bytes 2097184 | tf_op jit(solution)/shard_map/ppermute | solution.py:118
  397.9 8.9 %fusion.15 = bf16[256,4096]{1,0:T(8,128)(2,1)} fusion(bf16[1024,4096]{1,0:T(8,128)(2,1)} %constant_dynamic-update-slice_fusion.11, bf16[256,4096]{1,0:T(8,128)(2,1)} %collective-permute-done.23, bf16[256,4096]{1,0:T(8,128)(2,1)} %collective-permute-done.21, s32[]{:T(128)S(6)} %select_n.282, bf16[1024,512]{0,1:T(8,128)(2,1)S(1)} %fusion.29, ...), kind=kOutput, calls=%fused_computation.23 | convolution fusion | flops 2155872256 | bytes 16777220 | tf_op jit(solution)/shard_map/dot_general | solution.py:108
  (176 shorter events, 91.5 us)
Async XLA Ops:
  6.5 226.6 %all-gather.2.cloned.1.call-start = ((), (), s32[]{:S(2)}) async-start(), calls=%async_computation | async-start | bytes 11796480 | tf_op jit(solution)/shard_map/all_gather | solution.py:140
  9.1 14.5 %collective-permute-start.7 = (bf16[512,512]{1,0:T(8,128)(2,1)}, bf16[512,512]{1,0:T(8,128)(2,1)S(1)}, u32[]{:S(2)}, u32[]{:S(2)}) collective-permute-start(bf16[512,512]{1,0:T(8,128)(2,1)} %param.20), channel_id=1, source_target_pairs={{0,8},{8,16},{16,24},{24,28},{28,20},{20,12},{12,4},{4,0},{1,9},{9... | collective-permute-start | bytes 1572872 | tf_op jit(solution)/shard_map/ppermute | solution.py:91
  9.2 17.4 %collective-permute-start.14 = (bf16[512,512]{1,0:T(8,128)(2,1)}, bf16[512,512]{1,0:T(8,128)(2,1)S(1)}, u32[]{:S(2)}, u32[]{:S(2)}) collective-permute-start(bf16[512,512]{1,0:T(8,128)(2,1)} %param.21), channel_id=1, source_target_pairs={{8,0},{16,8},{24,16},{28,24},{20,28},{12,20},{4,12},{0,4},{9,1},{1... | collective-permute-start | bytes 1572872 | tf_op jit(solution)/shard_map/ppermute | solution.py:91
  11.2 117.8 %collective-permute-start = (bf16[1024,1024]{1,0:T(8,128)(2,1)}, bf16[1024,1024]{1,0:T(8,128)(2,1)}, u32[]{:S(2)}, u32[]{:S(2)}) collective-permute-start(bf16[1024,1024]{1,0:T(8,128)(2,1)} %param.11), channel_id=1, source_target_pairs={{0,2},{1,3},{2,0},{3,1},{4,6},{5,7},{6,4},{7,5},{8,10},{9,11},{10,... | collective-permute-start | bytes 6291464 | tf_op jit(solution)/shard_map/ppermute | solution.py:65
  12.7 184.5 %collective-permute-start.1 = (bf16[1024,1024]{1,0:T(8,128)(2,1)}, bf16[1024,1024]{1,0:T(8,128)(2,1)}, u32[]{:S(2)}, u32[]{:S(2)}) collective-permute-start(bf16[1024,1024]{1,0:T(8,128)(2,1)} %param.11), channel_id=1, source_target_pairs={{0,1},{1,0},{2,3},{3,2},{4,5},{5,4},{6,7},{7,6},{8,9},{9,8},{10,11... | collective-permute-start | bytes 6291464 | tf_op jit(solution)/shard_map/ppermute | solution.py:68
  23.6 38.7 %collective-permute-start.8 = (bf16[512,512]{1,0:T(8,128)(2,1)S(1)}, bf16[512,512]{1,0:T(8,128)(2,1)S(1)}, u32[]{:S(2)}, u32[]{:S(2)}) collective-permute-start(bf16[512,512]{1,0:T(8,128)(2,1)S(1)} %collective-permute-done.7), channel_id=1, source_target_pairs={{0,8},{8,16},{16,24},{24,28},{28,20},{20,12},{12,4},{4,0},{1,9},{9... | collective-permute-start | bytes 1572872 | tf_op jit(solution)/shard_map/ppermute | solution.py:91
  26.5 37.7 %collective-permute-start.15 = (bf16[512,512]{1,0:T(8,128)(2,1)S(1)}, bf16[512,512]{1,0:T(8,128)(2,1)S(1)}, u32[]{:S(2)}, u32[]{:S(2)}) collective-permute-start(bf16[512,512]{1,0:T(8,128)(2,1)S(1)} %collective-permute-done.14), channel_id=1, source_target_pairs={{8,0},{16,8},{24,16},{28,24},{20,28},{12,20},{4,12},{0,4},{9,1},{1... | collective-permute-start | bytes 1572872 | tf_op jit(solution)/shard_map/ppermute | solution.py:91
  62.4 25.4 %collective-permute-start.9 = (bf16[512,512]{1,0:T(8,128)(2,1)S(1)}, bf16[512,512]{1,0:T(8,128)(2,1)}, u32[]{:S(2)}, u32[]{:S(2)}) collective-permute-start(bf16[512,512]{1,0:T(8,128)(2,1)S(1)} %collective-permute-done.8), channel_id=1, source_target_pairs={{0,8},{8,16},{16,24},{24,28},{28,20},{20,12},{12,4},{4,0},{1,9},{9... | collective-permute-start | bytes 1572872 | tf_op jit(solution)/shard_map/ppermute | solution.py:91
  64.3 24.4 %collective-permute-start.16 = (bf16[512,512]{1,0:T(8,128)(2,1)S(1)}, bf16[512,512]{1,0:T(8,128)(2,1)}, u32[]{:S(2)}, u32[]{:S(2)}) collective-permute-start(bf16[512,512]{1,0:T(8,128)(2,1)S(1)} %collective-permute-done.15), channel_id=1, source_target_pairs={{8,0},{16,8},{24,16},{28,24},{20,28},{12,20},{4,12},{0,4},{9,1},{1... | collective-permute-start | bytes 1572872 | tf_op jit(solution)/shard_map/ppermute | solution.py:91
  87.7 23.9 %collective-permute-start.10 = (bf16[512,512]{1,0:T(8,128)(2,1)}, bf16[512,512]{1,0:T(8,128)(2,1)}, u32[]{:S(2)}, u32[]{:S(2)}) collective-permute-start(bf16[512,512]{1,0:T(8,128)(2,1)} %collective-permute-done.9), channel_id=1, source_target_pairs={{0,8},{8,16},{16,24},{24,28},{28,20},{20,12},{12,4},{4,0},{1,9},{9... | collective-permute-start | bytes 1572872 | tf_op jit(solution)/shard_map/ppermute | solution.py:91
  88.6 26.3 %collective-permute-start.17 = (bf16[512,512]{1,0:T(8,128)(2,1)}, bf16[512,512]{1,0:T(8,128)(2,1)}, u32[]{:S(2)}, u32[]{:S(2)}) collective-permute-start(bf16[512,512]{1,0:T(8,128)(2,1)} %collective-permute-done.16), channel_id=1, source_target_pairs={{8,0},{16,8},{24,16},{28,24},{20,28},{12,20},{4,12},{0,4},{9,1},{1... | collective-permute-start | bytes 1572872 | tf_op jit(solution)/shard_map/ppermute | solution.py:91
  111.6 42.8 %collective-permute-start.11 = (bf16[512,512]{1,0:T(8,128)(2,1)}, bf16[512,512]{1,0:T(8,128)(2,1)}, u32[]{:S(2)}, u32[]{:S(2)}) collective-permute-start(bf16[512,512]{1,0:T(8,128)(2,1)} %collective-permute-done.10), channel_id=1, source_target_pairs={{0,8},{8,16},{16,24},{24,28},{28,20},{20,12},{12,4},{4,0},{1,9},{9... | collective-permute-start | bytes 1572872 | tf_op jit(solution)/shard_map/ppermute | solution.py:91
  114.9 45.3 %collective-permute-start.18 = (bf16[512,512]{1,0:T(8,128)(2,1)}, bf16[512,512]{1,0:T(8,128)(2,1)}, u32[]{:S(2)}, u32[]{:S(2)}) collective-permute-start(bf16[512,512]{1,0:T(8,128)(2,1)} %collective-permute-done.17), channel_id=1, source_target_pairs={{8,0},{16,8},{24,16},{28,24},{20,28},{12,20},{4,12},{0,4},{9,1},{1... | collective-permute-start | bytes 1572872 | tf_op jit(solution)/shard_map/ppermute | solution.py:91
  128.9 100.6 %collective-permute-start.2 = (bf16[1024,1024]{1,0:T(8,128)(2,1)}, bf16[1024,1024]{1,0:T(8,128)(2,1)S(1)}, u32[]{:S(2)}, u32[]{:S(2)}) collective-permute-start(bf16[1024,1024]{1,0:T(8,128)(2,1)} %collective-permute-done), channel_id=1, source_target_pairs={{0,1},{1,0},{2,3},{3,2},{4,5},{5,4},{6,7},{7,6},{8,9},{9,8},{10,11... | collective-permute-start | bytes 6291464 | tf_op jit(solution)/shard_map/ppermute | solution.py:68
  154.4 40.8 %collective-permute-start.12 = (bf16[512,512]{1,0:T(8,128)(2,1)}, bf16[512,512]{1,0:T(8,128)(2,1)S(1)}, u32[]{:S(2)}, u32[]{:S(2)}) collective-permute-start(bf16[512,512]{1,0:T(8,128)(2,1)} %collective-permute-done.11), channel_id=1, source_target_pairs={{0,8},{8,16},{16,24},{24,28},{28,20},{20,12},{12,4},{4,0},{1,9},{9... | collective-permute-start | bytes 1572872 | tf_op jit(solution)/shard_map/ppermute | solution.py:91
  160.2 42.0 %collective-permute-start.19 = (bf16[512,512]{1,0:T(8,128)(2,1)}, bf16[512,512]{1,0:T(8,128)(2,1)S(1)}, u32[]{:S(2)}, u32[]{:S(2)}) collective-permute-start(bf16[512,512]{1,0:T(8,128)(2,1)} %collective-permute-done.18), channel_id=1, source_target_pairs={{8,0},{16,8},{24,16},{28,24},{20,28},{12,20},{4,12},{0,4},{9,1},{1... | collective-permute-start | bytes 1572872 | tf_op jit(solution)/shard_map/ppermute | solution.py:91
  195.2 24.3 %collective-permute-start.13 = (bf16[512,512]{1,0:T(8,128)(2,1)S(1)}, bf16[512,512]{1,0:T(8,128)(2,1)S(1)}, u32[]{:S(2)}, u32[]{:S(2)}) collective-permute-start(bf16[512,512]{1,0:T(8,128)(2,1)S(1)} %collective-permute-done.12), channel_id=1, source_target_pairs={{0,8},{8,16},{16,24},{24,28},{28,20},{20,12},{12,4},{4,0},{1,9},{9... | collective-permute-start | bytes 1572872 | tf_op jit(solution)/shard_map/ppermute | solution.py:91
  202.1 26.5 %collective-permute-start.20 = (bf16[512,512]{1,0:T(8,128)(2,1)S(1)}, bf16[512,512]{1,0:T(8,128)(2,1)S(1)}, u32[]{:S(2)}, u32[]{:S(2)}) collective-permute-start(bf16[512,512]{1,0:T(8,128)(2,1)S(1)} %collective-permute-done.19), channel_id=1, source_target_pairs={{8,0},{16,8},{24,16},{28,24},{20,28},{12,20},{4,12},{0,4},{9,1},{1... | collective-permute-start | bytes 1572872 | tf_op jit(solution)/shard_map/ppermute | solution.py:91
  263.2 35.6 %collective-permute-start.5 = (bf16[128,256]{1,0:T(8,128)(2,1)}, bf16[128,256]{1,0:T(8,128)(2,1)}, u32[]{:S(2)}, u32[]{:S(2)}) collective-permute-start(bf16[128,256]{1,0:T(8,128)(2,1)} %get-tuple-element.19), channel_id=1, source_target_pairs={{0,4},{4,8},{8,12},{12,16},{16,20},{20,24},{24,28},{1,5},{5,9},{9,... | collective-permute-start | bytes 196616 | tf_op jit(solution)/shard_map/ppermute | solution.py:24
  265.1 33.7 %collective-permute-start.6 = (bf16[128,256]{1,0:T(8,128)(2,1)}, bf16[128,256]{1,0:T(8,128)(2,1)}, u32[]{:S(2)}, u32[]{:S(2)}) collective-permute-start(bf16[128,256]{1,0:T(8,128)(2,1)} %get-tuple-element.20), channel_id=1, source_target_pairs={{4,0},{8,4},{12,8},{16,12},{20,16},{24,20},{28,24},{5,1},{9,5},{13... | collective-permute-start | bytes 196616 | tf_op jit(solution)/shard_map/ppermute | solution.py:27
  273.3 10.3 %collective-permute-start.3 = (bf16[8,512]{1,0:T(8,128)(2,1)}, bf16[8,512]{1,0:T(8,128)(2,1)S(1)}, u32[]{:S(2)}, u32[]{:S(2)}) collective-permute-start(bf16[8,512]{1,0:T(8,128)(2,1)} %get-tuple-element.7), channel_id=1, source_target_pairs={{0,4},{4,8},{8,12},{12,16},{16,20},{20,24},{24,28},{1,5},{5,9},{9,... | collective-permute-start | bytes 24584 | tf_op jit(solution)/shard_map/ppermute | solution.py:24
  334.3 7.7 %collective-permute-start.22 = (bf16[256,4096]{1,0:T(8,128)(2,1)}, bf16[256,4096]{1,0:T(8,128)(2,1)}, u32[]{:S(2)}, u32[]{:S(2)}) collective-permute-start(bf16[256,4096]{1,0:T(8,128)(2,1)} %convolution_convert_fusion), channel_id=1, source_target_pairs={{0,1},{1,0},{2,3},{3,2},{4,5},{5,4},{6,7},{7,6},{8,9},{9,8},{10,11... | collective-permute-start | bytes 6291464 | tf_op jit(solution)/shard_map/ppermute | solution.py:114
  341.5 10.0 %collective-permute-start.21 = (bf16[256,4096]{1,0:T(8,128)(2,1)}, bf16[256,4096]{1,0:T(8,128)(2,1)}, u32[]{:S(2)}, u32[]{:S(2)}) collective-permute-start(bf16[256,4096]{1,0:T(8,128)(2,1)} %convolution_convert_fusion.2), channel_id=1, source_target_pairs={{0,1},{1,0},{2,3},{3,2},{4,5},{5,4},{6,7},{7,6},{8,9},{9,8},{10,11... | collective-permute-start | bytes 6291464 | tf_op jit(solution)/shard_map/ppermute | solution.py:114
  350.0 47.9 %collective-permute-start.23 = (bf16[256,4096]{1,0:T(8,128)(2,1)}, bf16[256,4096]{1,0:T(8,128)(2,1)}, u32[]{:S(2)}, u32[]{:S(2)}) collective-permute-start(bf16[256,4096]{1,0:T(8,128)(2,1)} %fusion.16), channel_id=1, source_target_pairs={{0,2},{1,3},{2,0},{3,1},{4,6},{5,7},{6,4},{7,5},{8,10},{9,11},{10,... | collective-permute-start | bytes 6291464 | tf_op jit(solution)/shard_map/ppermute | solution.py:118
  (33 other events, 608.8 us)
Sparse Core Ops, SparseCore 0:
  9.5 208.0 all-gather.1
where the time goes:
time: 420 us; the launch traced here: 414 us
  waiting for transfers between devices  199 us (47%)
  matrix products  65.6 us (16%)
  local copies, waits for them, and re-layouts  54.1 us (13%)
  starting transfers between devices  41.9 us (10%)
  other arithmetic  39.1 us (9%)
  between operations  14.7 us (4%)
    ppermute x14, waiting for transfers between devices, ring_gather(): piece = lax.ppermute(piece, 'sp', perm)  152 us
    ppermute x1, waiting for transfers between devices, summed_over_tp(): arrived.append(lax.ppermute(both.astype(jnp.bfloat16), 'tp', perm))  46.3 us
    dot_general x4, matrix products, partial(): jnp.dot(piece, weight, preferred_element_type=jnp.float32)  31.4 us
    ppermute x14, starting transfers between devices, ring_gather(): piece = lax.ppermute(piece, 'sp', perm)  25.8 us
    dynamic_update_slice x14, local copies, waits for them, and re-layouts, ring_gather(): whole = lax.dynamic_update_slice(whole, piece, starts)  20.6 us
    dot_general x1, matrix products, shards(): raw = jnp.dot(normed, in_full, preferred_element_type=jnp.float32)  17.8 us
    reduce_sum x1, other arithmetic, shards(): jnp.sum(expo, axis=-1, keepdims=True) + jnp.exp(sink - highest)  9.5 us
    another operation x7, other arithmetic  9.15 us
  transfers between devices with their start and end apart: 25, of which 9 were waited for; matrix products, arithmetic and copies ran while one was open for 19% of the time, Pallas kernels for 0%

commit v1 on v0

v1 whole, which is shorter than its diff:
```python
import functools

import jax
import jax.numpy as jnp
import numpy as np
from jax import lax
from jax.experimental import pallas as pl
from jax.experimental.pallas import tpu as pltpu
from jax.sharding import PartitionSpec as P

HEAD_DIM = 64
Q_HEADS = 32
KV_HEADS = 8
GROUP_DIM = 256
WINDOW = 128
GRID_W = 64
LANES = 128
SUBS = 4
CHUNKS = 4
POOL_PAD = 16
LAG = 5

epsilon = 1e-06
rotary_base = 10000.0
masked_score = -1e30
MESH = pl.DeviceIdType.MESH


def rotary_tables(total_rows):
    freq_count = HEAD_DIM // 4
    inverse = np.float32(rotary_base) ** (-np.arange(freq_count, dtype=np.float32) / np.float32(freq_count))
    lane = np.arange(LANES)
    dim = lane % HEAD_DIM
    by_col = (dim // (HEAD_DIM // 2)) == 1
    is_b = (dim % (HEAD_DIM // 2)) // freq_count == 1
    freq = inverse[dim % freq_count]
    sign = np.where(is_b, np.float32(1.0), np.float32(-1.0))
    tables = []
    for count, mine in ((total_rows // GRID_W, ~by_col), (GRID_W, by_col)):
        angle = np.arange(count, dtype=np.float32)[:, None] * freq[None, :]
        tables.append(np.where(mine, np.cos(angle), np.float32(0.0)).astype(np.float32))
        tables.append(np.where(mine, np.sin(angle) * sign, np.float32(0.0)).astype(np.float32))
    return tables


def spread_matrix(kv_width):
    heads = kv_width // HEAD_DIM
    spread = np.zeros((2 * kv_width, 4 * heads * LANES), np.float32)
    for kind in range(2):
        for head in range(heads):
            for half in range(2):
                block = (kind * heads + head) * 2 + half
                for d in range(HEAD_DIM):
                    spread[kind * kv_width + head * HEAD_DIM + d, block * LANES + half * HEAD_DIM + d] = 1.0
    return spread


def layer_kernel(
    dims,
    tokens,
    pool_in_w,
    query_w,
    kv_parts,
    out_pool_w,
    out_attn_w,
    gain,
    pool_w,
    pool_scale,
    sink,
    row_cos,
    row_sin,
    col_cos,
    col_sin,
    spread,
    out,
    tok,
    in_w,
    out_w,
    acc,
    queries,
    pool_pad,
    kv,
    kvx,
    mixers,
    to_core,
    own_sum,
    from_core,
    from_chip,
    load_sem,
    in_send,
    in_recv,
    ow_send,
    ow_recv,
    tx_send,
    tx_recv,
    td_send,
    td_recv,
    halo_send,
    halo_recv,
    core_send,
    core_recv,
    chip_send,
    chip_recv,
):
    n_sp, n_tp = dims["sp"], dims["tp"]
    rows, feats = tokens.shape
    depth = pool_in_w.shape[0]
    pool_ch = pool_in_w.shape[1]
    q_width = query_w.shape[1]
    kvw = dims["kvw"]
    cols_dev = out_pool_w.shape[1]
    nq = dims["nq"]
    nr = SUBS // nq
    col_q = cols_dev // nq
    half = n_sp // 2
    chips = n_tp // 2
    part_rows = rows // n_tp
    pieces = n_sp * nq

    sp = lax.axis_index("sp")
    tp = lax.axis_index("tp")
    chip = tp // 2
    core = tp % 2
    place = jnp.where(sp % 2 == 0, sp // 2, n_sp - 1 - sp // 2)

    def owner_at(spot):
        spot = (spot + n_sp) % n_sp
        return jnp.where(spot < half, 2 * spot, 2 * (n_sp - 1 - spot) + 1)

    ahead = (owner_at(place + 1), tp)
    behind = (owner_at(place - 1), tp)
    partner = (sp, chip * 2 + 1 - core)

    def chip_peer(rel):
        return (sp, ((chip + rel) % chips) * 2 + core)

    def source_slot(rel):
        return ((chip - rel + chips) % chips) * 2 + core

    barrier = pltpu.get_barrier_semaphore()
    greeted = [ahead, behind, ((sp + 1) % n_sp, tp), ((sp + n_sp - 1) % n_sp, tp), partner]
    greeted += [chip_peer(rel) for rel in range(1, chips)]
    for other in greeted:
        pl.semaphore_signal(barrier, inc=1, device_id=other, device_id_type=MESH)

    loads = []

    def load(src, dst):
        copy = pltpu.make_async_copy(src, dst, load_sem.at[len(loads)])
        copy.start()
        loads.append(copy)

    load(pool_in_w, in_w.at[sp, :, pl.ds(0, pool_ch)])
    load(query_w, in_w.at[sp, :, pl.ds(pool_ch, q_width)])
    start = pool_ch + q_width
    for part in kv_parts:
        load(part, in_w.at[sp, :, pl.ds(start, part.shape[1])])
        start += part.shape[1]
    in_loads = len(loads)
    load(tokens, tok.at[tp])
    for q in range(nq):
        load(out_pool_w.at[:, pl.ds(q * col_q, col_q)], out_w.at[sp, q, pl.ds(0, pool_ch)])
        load(out_attn_w.at[:, pl.ds(q * col_q, col_q)], out_w.at[sp, q, pl.ds(pool_ch, q_width)])

    def in_sub(owner, u):
        return in_w.at[owner, pl.ds(u * (depth // SUBS), depth // SUBS)]

    out_rows = pool_ch + q_width

    def out_sub(owner, u):
        return out_w.at[owner, u // nr, pl.ds((u % nr) * (out_rows // nr), out_rows // nr)]

    def ring_copy(sub, sems, d, s, u):
        owner = owner_at(place - (s - 1) if d == 0 else place + (s - 1))
        ref = sub(owner, u)
        return pltpu.make_async_remote_copy(
            src_ref=ref,
            dst_ref=ref,
            send_sem=sems[0].at[d, s - 1, u],
            recv_sem=sems[1].at[d, s - 1, u],
            device_id=ahead if d == 0 else behind,
            device_id_type=MESH,
        )

    def ring_arrived(sub, sems, d, s, u):
        owner = owner_at(place - s if d == 0 else place + s)
        ref = sub(owner, u)
        pltpu.make_async_remote_copy(
            src_ref=ref,
            dst_ref=ref,
            send_sem=sems[0].at[d, s - 1, u],
            recv_sem=sems[1].at[d, s - 1, u],
            device_id=behind if d == 0 else ahead,
            device_id_type=MESH,
        ).wait_recv()

    in_ring = (in_sub, (in_send, in_recv))
    ow_ring = (out_sub, (ow_send, ow_recv))

    def ring_start(ring, subs):
        for u in subs:
            for d in range(2):
                ring_copy(*ring, d, 1, u).start()

    def in_half(d, u):
        return u < SUBS // 2 if d == 0 else u >= SUBS // 2

    def ring_step(ring, s, u, last):
        for d in range(2):
            ring_arrived(*ring, d, s, u)
            if not last or in_half(d, u):
                ring_copy(*ring, d, s + 1, u).start()

    def ring_last(ring, k):
        ring_arrived(*ring, 0, half, k)
        ring_arrived(*ring, 1, half, SUBS // 2 + k)

    def ring_sent(ring):
        def full(s, carry):
            for u in range(SUBS):
                for d in range(2):
                    ring_copy(*ring, d, s, u).wait_send()
            return carry

        lax.fori_loop(1, half, full, 0)
        for u in range(SUBS):
            ring_copy(*ring, 0 if in_half(0, u) else 1, half, u).wait_send()

    chunk = rows // CHUNKS

    def tok_rows(slot, j):
        return tok.at[slot, pl.ds(j * chunk, chunk)]

    def over_chips(rel, j, slot):
        return pltpu.make_async_remote_copy(
            src_ref=tok_rows(slot, j),
            dst_ref=tok_rows(slot, j),
            send_sem=tx_send.at[rel - 1, j],
            recv_sem=tx_recv.at[rel - 1, j],
            device_id=chip_peer(rel),
            device_id_type=MESH,
        )

    def over_cores(rel, j, slot):
        return pltpu.make_async_remote_copy(
            src_ref=tok_rows(slot, j),
            dst_ref=tok_rows(slot, j),
            send_sem=td_send.at[rel, j],
            recv_sem=td_recv.at[rel, j],
            device_id=partner,
            device_id_type=MESH,
        )

    pl.semaphore_wait(barrier, len(greeted))
    for copy in loads[:in_loads]:
        copy.wait()
    ring_start(in_ring, range(SUBS))
    loads[in_loads].wait()
    for j in range(CHUNKS):
        for rel in range(1, chips):
            over_chips(rel, j, tp).start()
        over_cores(0, j, tp).start()
    acc[...] = jnp.zeros_like(acc)
    for copy in loads[in_loads + 1 :]:
        copy.wait()

    @pl.when(sp == 0)
    def _():
        kv[pl.ds(0, WINDOW)] = jnp.zeros((WINDOW, kv.shape[1]), kv.dtype)
        pool_pad[pl.ds(0, POOL_PAD)] = jnp.zeros((POOL_PAD, pool_ch), pool_pad.dtype)

    @pl.when(sp == n_sp - 1)
    def _():
        kv[pl.ds(WINDOW + rows, WINDOW)] = jnp.zeros((WINDOW, kv.shape[1]), kv.dtype)
        pool_pad[pl.ds(POOL_PAD + rows, POOL_PAD)] = jnp.zeros((POOL_PAD, pool_ch), pool_pad.dtype)

    def pass_tokens(j):
        for rel in range(1, chips):
            over_chips(rel, j, source_slot(rel)).wait_recv()
            over_cores(rel, j, source_slot(rel)).start()

    norm_rows = 32

    def normalise(j):
        for rel in range(chips):
            slot = source_slot(rel)
            over_cores(rel, j, (slot // 2) * 2 + 1 - core).wait_recv()
            over_cores(rel, j, slot).wait_send()
            if rel:
                over_chips(rel, j, tp).wait_send()

        def tile(i, carry):
            at = pl.ds(pl.multiple_of(j * chunk + i * norm_rows, norm_rows), norm_rows)
            total = jnp.zeros((norm_rows, 1), jnp.float32)
            for slot in range(n_tp):
                floats = tok[slot, at, :].astype(jnp.float32)
                total = total + jnp.sum(floats * floats, axis=-1, keepdims=True)
            scale = lax.rsqrt(total / (feats * n_tp) + epsilon)
            for slot in range(n_tp):
                floats = tok[slot, at, :].astype(jnp.float32)
                tok[slot, at, :] = ((floats * scale) * gain[slot]).astype(jnp.bfloat16)
            return carry

        lax.fori_loop(0, chunk // norm_rows, tile, 0)

    mm_rows = min(rows, 512)

    def block_owner(i):
        return owner_at(place + jnp.where(i % 2 == 1, -((i + 1) // 2), i // 2))

    def project(first, last):
        def step(k, carry):
            i, tile = k // (rows // mm_rows), k % (rows // mm_rows)
            owner = block_owner(i)
            at = pl.ds(pl.multiple_of(tile * mm_rows, mm_rows), mm_rows)
            offset = owner * depth
            part = tok[offset // feats, at, pl.ds(pl.multiple_of(offset % feats, depth), depth)]
            acc[at, :] += jnp.dot(part, in_w[owner], preferred_element_type=jnp.float32)
            return carry

        lax.fori_loop(first * (rows // mm_rows), last * (rows // mm_rows), step, 0)

    ring_step(in_ring, 1, 0, False)
    pass_tokens(0)
    ring_step(in_ring, 1, 1, False)
    normalise(0)
    ring_step(in_ring, 1, 2, False)
    pass_tokens(1)
    ring_step(in_ring, 1, 3, False)
    normalise(1)
    pass_tokens(2)
    ring_step(in_ring, 2, 0, half == 3)
    normalise(2)
    ring_step(in_ring, 2, 1, half == 3)
    pass_tokens(3)
    ring_step(in_ring, 2, 2, half == 3)
    normalise(3)
    project(0, 3)
    ring_step(in_ring, 2, 3, half == 3)
    project(3, 5)

    def middle_in(s, carry):
        for u in range(SUBS):
            ring_step(in_ring, s, u, False)
        project(2 * s - 1, 2 * s + 1)
        return carry

    if half > 4:
        lax.fori_loop(3, half - 1, middle_in, 0)
    if half > 3:
        for u in range(SUBS):
            ring_step(in_ring, half - 1, u, True)
        ring_start(ow_ring, range(SUBS // 2))
        project(n_sp - 3, n_sp - 1)
    for k in range(SUBS // 2):
        ring_last(in_ring, k)
    project(n_sp - 1, n_sp)

    lane = lax.broadcasted_iota(jnp.int32, (GRID_W, LANES), 1)
    take_next = (lane % (HEAD_DIM // 2)) < HEAD_DIM // 4
    kv_cols = 2 * kvw

    def turn(i, carry):
        at = pl.ds(pl.multiple_of(i * GRID_W, GRID_W), GRID_W)
        grid_row = sp * (rows // GRID_W) + i
        cosine = row_cos[pl.ds(grid_row, 1), :] + col_cos[...]
        sine = row_sin[pl.ds(grid_row, 1), :] + col_sin[...]
        to = pl.ds(pl.multiple_of(POOL_PAD + i * GRID_W, POOL_PAD), GRID_W)
        pool_pad[to, :] = acc[at, pl.ds(0, pool_ch)].astype(jnp.bfloat16)

        def turned(start):
            raw = acc[at, pl.ds(start, LANES)]
            other = jnp.where(
                take_next,
                pltpu.roll(raw, LANES - HEAD_DIM // 4, 1),
                pltpu.roll(raw, HEAD_DIM // 4, 1),
            )
            return raw, raw * cosine + other * sine

        for slab in range(q_width // LANES):
            _, values = turned(pool_ch + slab * LANES)
            queries[at, pl.ds(slab * LANES, LANES)] = (values * HEAD_DIM ** (-0.5)).astype(jnp.bfloat16)
        to = pl.ds(pl.multiple_of(WINDOW + i * GRID_W, GRID_W), GRID_W)
        for slab in range(kv_cols // LANES):
            begin = pool_ch + q_width + slab * LANES
            turn_lanes = max(0, min(LANES, kvw - slab * LANES))
            if turn_lanes == 0:
                values = acc[at, pl.ds(begin, LANES)]
            else:
                raw, values = turned(begin)
                if turn_lanes < LANES:
                    values = jnp.where(lane < turn_lanes, values, raw)
            kv[to, pl.ds(slab * LANES, LANES)] = values.astype(jnp.bfloat16)
        return carry

    lax.fori_loop(0, rows // GRID_W, turn, 0)

    def halo(k, up):
        ref, width = ((kv, WINDOW), (pool_pad, POOL_PAD))[k]
        src = pl.ds(rows if up else width, width)
        dst = pl.ds(0 if up else rows + width, width)
        other = ((sp + 1) % n_sp if up else (sp + n_sp - 1) % n_sp, tp)
        return pltpu.make_async_remote_copy(
            src_ref=ref.at[src],
            dst_ref=ref.at[dst],
            send_sem=halo_send.at[k, int(up)],
            recv_sem=halo_recv.at[k, int(up)],
            device_id=other,
            device_id_type=MESH,
        )

    @pl.when(sp < n_sp - 1)
    def _():
        for k in range(2):
            halo(k, True).start()

    @pl.when(sp > 0)
    def _():
        for k in range(2):
            halo(k, False).start()

    ring_start(ow_ring, range(SUBS // 2, SUBS))

    def spread_rows(start, count):
        at = pl.ds(start, count)
        kvx[at, :] = jnp.dot(kv[at, :], spread[...], preferred_element_type=jnp.float32).astype(jnp.bfloat16)

    def spread_tile(i, carry):
        spread_rows(pl.multiple_of((i + 1) * WINDOW, WINDOW), WINDOW)
        return carry

    lax.fori_loop(0, rows // WINDOW, spread_tile, 0)

    span = 3 * WINDOW
    heads_kv = kvw // HEAD_DIM
    group = Q_HEADS // KV_HEADS
    blocks = rows // WINDOW

    def variant(kind, head, upper):
        return pl.ds(((kind * heads_kv + head) * 2 + upper) * LANES, LANES)

    def attend(i, carry):
        at = pl.ds(pl.multiple_of(i * WINDOW, WINDOW), WINDOW)
        keys_at = pl.ds(pl.multiple_of(i * WINDOW, WINDOW), span)
        query = lax.broadcasted_iota(jnp.int32, (WINDOW, span), 0)
        key = lax.broadcasted_iota(jnp.int32, (WINDOW, span), 1)
        low = jnp.where((sp == 0) & (i == 0), WINDOW, 0)
        high = jnp.where((sp == n_sp - 1) & (i == blocks - 1), 2 * WINDOW, span)
        allowed = (key >= jnp.maximum(query, low)) & (key <= jnp.minimum(query + 2 * WINDOW, high - 1))
        for head in range(heads_kv):
            for pair in range(group // 2):
                slab = head * (group // 2) + pair
                q_pair = queries[at, pl.ds(slab * LANES, LANES)]
                result = jnp.zeros((WINDOW, LANES), jnp.float32)
                for upper in range(2):
                    scores = lax.dot_general(
                        q_pair,
                        kvx[keys_at, variant(0, head, upper)],
                        (((1,), (1,)), ((), ())),
                        preferred_element_type=jnp.float32,
                    )
                    scores = jnp.where(allowed, scores, masked_score)
                    logit = sink[slab * 2 + upper]
                    highest = jnp.maximum(jnp.max(scores, axis=-1, keepdims=True), logit)
                    expo = jnp.exp(scores - highest)
                    denominator = jnp.sum(expo, axis=-1, keepdims=True) + jnp.exp(logit - highest)
                    weights = (expo * (1.0 / denominator)).astype(jnp.bfloat16)
                    result += jnp.dot(
                        weights, kvx[keys_at, variant(1, head, upper)], preferred_element_type=jnp.float32
                    )
                mixers[at, pl.ds(pool_ch + slab * LANES, LANES)] = result.astype(jnp.bfloat16)
        return carry

    lax.fori_loop(1, blocks - 1, attend, 0)
    for u in range(2):
        ring_step(ow_ring, 1, u, False)

    @pl.when(sp > 0)
    def _():
        for k in range(2):
            halo(k, True).wait_recv()

    @pl.when(sp < n_sp - 1)
    def _():
        for k in range(2):
            halo(k, False).wait_recv()

    spread_rows(0, WINDOW)
    spread_rows(WINDOW + rows, WINDOW)
    lax.fori_loop(0, 2, lambda e, carry: attend(e * (blocks - 1), carry), 0)
    ring_step(ow_ring, 1, 2, False)

    groups_dev = pool_ch // GROUP_DIM
    tile_rows = 256

    def pool_tile(i, carry):
        at = pl.ds(pl.multiple_of(i * tile_rows, tile_rows), tile_rows)
        wide = tile_rows + 2 * POOL_PAD
        row = lax.broadcasted_iota(jnp.int32, (tile_rows, wide), 0)
        rel = lax.broadcasted_iota(jnp.int32, (tile_rows, wide), 1) - POOL_PAD - row
        position = sp * rows + i * tile_rows + lax.broadcasted_iota(jnp.int32, (tile_rows, LANES), 0)
        for g in range(groups_dev):
            level = (tp * groups_dev + g) % 4
            reach = jnp.where(level == 0, 1, jnp.where(level == 1, 2, jnp.where(level == 2, 4, 8)))
            band = jnp.where((rel >= -reach) & (rel < reach), 1.0, 0.0).astype(jnp.bfloat16)
            cols = pl.ds(g * GROUP_DIM, GROUP_DIM)
            around = pool_pad[pl.ds(pl.multiple_of(i * tile_rows, tile_rows), wide), cols]
            here = pool_pad[pl.ds(pl.multiple_of(i * tile_rows + POOL_PAD, POOL_PAD), tile_rows), cols]
            window_sum = jnp.dot(band, around, preferred_element_type=jnp.float32)
            count = jnp.minimum(position + reach, n_sp * rows) - jnp.maximum(position - reach, 0)
            count = jnp.concatenate([count.astype(jnp.float32)] * (GROUP_DIM // LANES), axis=1)
            pooled = (window_sum / count - here.astype(jnp.float32)).astype(jnp.bfloat16)
            mixed = jnp.dot(pooled, pool_w[g], preferred_element_type=jnp.float32)
            mixers[at, cols] = (mixed * pool_scale[:, cols]).astype(jnp.bfloat16)
        return carry

    lax.fori_loop(0, rows // tile_rows, pool_tile, 0)
    ring_step(ow_ring, 1, 3, False)

    def piece_at(m):
        later = m - nq
        s = later // (2 * nq) + 1
        r = later - (s - 1) * (2 * nq)
        final = s == half
        q = jnp.where(final, r, r // 2)
        delta = jnp.where(final | (r % 2 == 0), -s, s)
        own = m < nq
        return owner_at(place + jnp.where(own, 0, delta)), jnp.where(own, m, q)

    def core_copy(m):
        return pltpu.make_async_remote_copy(
            src_ref=to_core.at[m],
            dst_ref=from_core.at[m],
            send_sem=core_send.at[m],
            recv_sem=core_recv.at[m],
            device_id=partner,
            device_id_type=MESH,
        )

    def chip_copy(m, rel):
        return pltpu.make_async_remote_copy(
            src_ref=own_sum.at[m, (chip + rel) % chips],
            dst_ref=from_chip.at[m, rel - 1],
            send_sem=chip_send.at[m, rel - 1],
            recv_sem=chip_recv.at[m, rel - 1],
            device_id=chip_peer(rel),
            device_id_type=MESH,
        )

    def multiply(m):
        owner, q = piece_at(m)
        for mine, target in ((1 - core, to_core), (core, own_sum)):

            def part(c, carry, mine=mine, target=target):
                at = pl.ds(pl.multiple_of((2 * c + mine) * part_rows, part_rows), part_rows)
                target[m, c] = jnp.dot(
                    mixers[at, :], out_w[owner, q], preferred_element_type=jnp.float32
                ).astype(jnp.bfloat16)
                return carry

            lax.fori_loop(0, chips, part, 0)
            if target is to_core:
                core_copy(m).start()

    def pass_sum(m):
        core_copy(m).wait_recv()
        for rel in range(1, chips):
            c = (chip + rel) % chips
            both = own_sum[m, c].astype(jnp.float32) + from_core[m, c].astype(jnp.float32)
            own_sum[m, c] = both.astype(jnp.bfloat16)
            chip_copy(m, rel).start()

    def total(m):
        owner, q = piece_at(m)
        value = own_sum[m, chip].astype(jnp.float32) + from_core[m, chip].astype(jnp.float32)
        for rel in range(1, chips):
            chip_copy(m, rel).wait_recv()
            value = value + from_chip[m, rel - 1].astype(jnp.float32)
        out[:, pl.ds(pl.multiple_of(owner * cols_dev + q * col_q, col_q), col_q)] = value.astype(out.dtype)

    def piece(m, carry):
        multiply(m)

        @pl.when(m > 0)
        def _():
            pass_sum(m - 1)

        @pl.when(m >= LAG)
        def _():
            total(m - LAG)

        return carry

    lax.fori_loop(0, 3 * nq, piece, 0)

    def out_step(s, last):
        for u in range(SUBS):
            ring_step(ow_ring, s, u, last)
            if (u + 1) % nr == 0:
                first = nq + (s - 1) * 2 * nq + 2 * (u // nr)
                lax.fori_loop(first, first + 2, piece, 0)

    def middle_out(s, carry):
        out_step(s, False)
        return carry

    lax.fori_loop(2, half - 1, middle_out, 0)
    out_step(half - 1, True)
    for k in range(SUBS // 2):
        ring_last(ow_ring, k)
    lax.fori_loop(pieces - nq, pieces, piece, 0)
    pass_sum(pieces - 1)

    def finish(m, carry):
        total(m)
        return carry

    lax.fori_loop(pieces - LAG, pieces, finish, 0)

    ring_sent(in_ring)
    ring_sent(ow_ring)

    @pl.when(sp < n_sp - 1)
    def _():
        for k in range(2):
            halo(k, True).wait_send()

    @pl.when(sp > 0)
    def _():
        for k in range(2):
            halo(k, False).wait_send()

    def sums_sent(m, carry):
        core_copy(m).wait_send()
        for rel in range(1, chips):
            chip_copy(m, rel).wait_send()
        return carry

    lax.fori_loop(0, pieces, sums_sent, 0)


def shards(
    n_sp,
    n_tp,
    tokens,
    norm_gain,
    pool_in_weight,
    query_weight,
    key_weight,
    value_weight,
    pool_weight,
    pool_scale,
    sink_logit,
    out_pool_weight,
    out_attn_weight,
):
    rows, feats = tokens.shape
    depth, pool_ch = pool_in_weight.shape
    q_width = query_weight.shape[1]
    kvw = key_weight.shape[1]
    cols_dev = out_pool_weight.shape[1]
    in_cols = pool_ch + q_width + 2 * kvw
    out_rows = pool_ch + q_width
    half = n_sp // 2
    chips = n_tp // 2
    nq = 2 if cols_dev >= 2 * LANES else 1
    col_q = cols_dev // nq
    pieces = n_sp * nq
    part_rows = rows // n_tp
    if kvw % LANES:
        kv_parts = (jnp.concatenate([key_weight, value_weight], axis=1),)
    else:
        kv_parts = (key_weight, value_weight)
    tables = [jnp.asarray(t) for t in rotary_tables(rows * n_sp)]
    spread = jnp.asarray(spread_matrix(kvw), jnp.bfloat16)
    dims = dict(sp=n_sp, tp=n_tp, kvw=kvw, nq=nq)
    count = len(kv_parts)

    def kernel(*refs):
        layer_kernel(dims, *refs[:3], refs[3 : 3 + count], *refs[3 + count :])

    anywhere = pl.BlockSpec(memory_space=pl.ANY)
    vmem = pl.BlockSpec(memory_space=pltpu.VMEM)
    smem = pl.BlockSpec(memory_space=pltpu.SMEM)
    bf16, f32, dma = jnp.bfloat16, jnp.float32, pltpu.SemaphoreType.DMA
    return pl.pallas_call(
        kernel,
        out_shape=jax.ShapeDtypeStruct((rows // n_tp, cols_dev * n_sp), bf16),
        in_specs=[anywhere] * (5 + count) + [vmem] * 3 + [smem] + [vmem] * 5,
        out_specs=vmem,
        scratch_shapes=[
            pltpu.VMEM((n_tp, rows, feats), bf16),
            pltpu.VMEM((n_sp, depth, in_cols), bf16),
            pltpu.VMEM((n_sp, nq, out_rows, col_q), bf16),
            pltpu.VMEM((rows, in_cols), f32),
            pltpu.VMEM((rows, q_width), bf16),
            pltpu.VMEM((rows + 2 * POOL_PAD, pool_ch), bf16),
            pltpu.VMEM((rows + 2 * WINDOW, 2 * kvw), bf16),
            pltpu.VMEM((rows + 2 * WINDOW, 4 * (kvw // HEAD_DIM) * LANES), bf16),
            pltpu.VMEM((rows, out_rows), bf16),
            pltpu.VMEM((pieces, chips, part_rows, col_q), bf16),
            pltpu.VMEM((pieces, chips, part_rows, col_q), bf16),
            pltpu.VMEM((pieces, chips, part_rows, col_q), bf16),
            pltpu.VMEM((pieces, chips - 1, part_rows, col_q), bf16),
            dma((2 + count + 1 + 2 * nq,)),
            dma((2, half, SUBS)),
            dma((2, half, SUBS)),
            dma((2, half, SUBS)),
            dma((2, half, SUBS)),
            dma((chips - 1, CHUNKS)),
            dma((chips - 1, CHUNKS)),
            dma((chips, CHUNKS)),
            dma((chips, CHUNKS)),
            dma((2, 2)),
            dma((2, 2)),
            dma((pieces,)),
            dma((pieces,)),
            dma((pieces, chips - 1)),
            dma((pieces, chips - 1)),
        ],
        compiler_params=pltpu.CompilerParams(
            collective_id=0, has_side_effects=True, vmem_limit_bytes=67043328
        ),
        name="layer",
    )(
        tokens,
        pool_in_weight,
        query_weight,
        *kv_parts,
        out_pool_weight,
        out_attn_weight,
        norm_gain.reshape(n_tp, 1, feats),
        pool_weight,
        pool_scale.reshape(1, pool_ch),
        sink_logit,
        *tables,
        spread,
    )


def solution(mesh):
    return jax.shard_map(
        functools.partial(shards, mesh.shape["sp"], mesh.shape["tp"]),
        mesh=mesh,
        in_specs=(
            P("sp", "tp"),
            P(),
            P("sp", "tp"),
            P("sp", "tp"),
            P("sp", "tp"),
            P("sp", "tp"),
            P("tp", None, None),
            P("tp"),
            P("tp"),
            P("tp", "sp"),
            P("tp", "sp"),
        ),
        out_specs=P(("sp", "tp"), None),
        check_vma=False,
    )
```

time: 420 us -> 206 us (0.49); the launches traced: 414 us -> 205 us
  Pallas kernels: 0 us -> 202 us
  waiting for transfers between devices: 199 us -> 0 us
  matrix products: 65.6 us -> 0 us
  local copies, waits for them, and re-layouts: 54.1 us -> 3.13 us
  starting transfers between devices: 41.9 us -> 0 us
  other arithmetic: 39.1 us -> 0 us
  between operations: 14.7 us -> 0.01 us
    pallas_call x0 -> x1, Pallas kernels: none -> 202 us  [shards(): pl.pallas_call(kernel, out_shape=jax.ShapeDtypeStruct((rows // n_tp, cols...]
    ppermute x24 -> x0, waiting for transfers between devices: 199 us -> none  [the longest x14 152 us: ring_gather(): piece = lax.ppermute(piece, 'sp', perm)]
    dot_general x8 -> x0, matrix products: 65.6 us -> none  [the longest x4 31.4 us: partial(): jnp.dot(piece, weight, preferred_element_type=jnp.float32)]
    ppermute x24 -> x0, starting transfers between devices: 41.9 us -> none  [the longest x14 25.8 us: ring_gather(): piece = lax.ppermute(piece, 'sp', perm)]
    dynamic_update_slice x18 -> x0, local copies, waits for them, and re-layouts: 27.3 us -> none  [the longest x14 20.6 us: ring_gather(): whole = lax.dynamic_update_slice(whole, piece, starts)]
    reduce_sum x2 -> x0, other arithmetic: 11.2 us -> none  [the longest x1 9.5 us: shards(): jnp.sum(expo, axis=-1, keepdims=True) + jnp.exp(sink - highest)]
    another operation x10 -> x0, other arithmetic: 10.7 us -> none
    another operation x6 -> x0, local copies, waits for them, and re-layouts: 7.13 us -> none
  transfers between devices with their start and end apart: 25 -> 0, of which waited for: 9 -> 0; matrix products, arithmetic and copies ran while one was open for 19% -> 0% of each run, Pallas kernels for 0% -> 0%
where the time goes in v1:
time: 206 us; the launch traced here: 205 us
  Pallas kernels  202 us (98%)
  local copies, waits for them, and re-layouts  3.13 us (2%)
    pallas_call x1, Pallas kernels, shards(): pl.pallas_call(kernel, out_shape=jax.ShapeDtypeStruct((rows // n_tp, cols...  202 us

profile of v1, /device:TPU:4, one launch (start us, length us, event | category | flops | bytes accessed | tf_op | source)
XLA Modules:
  0.0 205.4 jit_solution(7152998841717154573)
XLA Ops:
  0.0 202.2 %layer.1 = bf16[256,4096]{1,0:T(8,128)(2,1)} custom-call(bf16[1024,1024]{1,0:T(8,128)(2,1)} %refs_0_.1, bf16[512,512]{1,0:T(8,128)(2,1)} %refs_1_.1, bf16[512,512]{1,0:T(8,128)(2,1)} %refs_2_.1, bf16[512,128]{1,0:T(8,128)(2,1)} %refs_3_.1, bf16[512,128]{1,0:T(8,128)(2,1)} %refs_4_.1, bf16[512,512]{1,0:T(8,128)(2,1)} %refs_5_.1, bf16[512,512]{1,0:T(8,128)(2,1)} %refs_6_.1, ...), custom_call_target="tpu_custom_call" | custom-call | tf_op jit(solution)/shard_map/layer/pallas_call | solution.py:686
  202.2 3.1 %copy.18 = bf16[256,4096]{1,0:T(8,128)(2,1)} copy(bf16[256,4096]{1,0:T(8,128)(2,1)} %layer.1) | data formatting | bytes 4194304

commit v2 on v1

--- a/solution.py
+++ b/solution.py
@@ -18,7 +18,7 @@
 SUBS = 4
 CHUNKS = 4
 POOL_PAD = 16
-LAG = 5
+LAG = 3
 
 epsilon = 1e-06
 rotary_base = 10000.0
@@ -63,15 +63,8 @@
     kv_parts,
     out_pool_w,
     out_attn_w,
-    gain,
-    pool_w,
-    pool_scale,
+    small_refs,
     sink,
-    row_cos,
-    row_sin,
-    col_cos,
-    col_sin,
-    spread,
     out,
     tok,
     in_w,
@@ -86,6 +79,14 @@
     own_sum,
     from_core,
     from_chip,
+    gain,
+    pool_w,
+    pool_scale,
+    row_cos,
+    row_sin,
+    col_cos,
+    col_sin,
+    spread,
     load_sem,
     in_send,
     in_recv,
@@ -110,6 +111,7 @@
     kvw = dims["kvw"]
     cols_dev = out_pool_w.shape[1]
     nq = dims["nq"]
+    wide = dims["wide"]
     nr = SUBS // nq
     col_q = cols_dev // nq
     half = n_sp // 2
@@ -150,17 +152,22 @@
         copy.start()
         loads.append(copy)
 
-    load(pool_in_w, in_w.at[sp, :, pl.ds(0, pool_ch)])
-    load(query_w, in_w.at[sp, :, pl.ds(pool_ch, q_width)])
-    start = pool_ch + q_width
-    for part in kv_parts:
-        load(part, in_w.at[sp, :, pl.ds(start, part.shape[1])])
-        start += part.shape[1]
-    in_loads = len(loads)
+    sub_rows = depth // SUBS
+    for u in range(SUBS):
+        at = pl.ds(u * sub_rows, sub_rows)
+        start = 0
+        for part in (pool_in_w, query_w, *kv_parts):
+            load(part.at[at], in_w.at[sp, at, pl.ds(start, part.shape[1])])
+            start += part.shape[1]
+    in_loads = len(loads) // SUBS
     load(tokens, tok.at[tp])
-    for q in range(nq):
-        load(out_pool_w.at[:, pl.ds(q * col_q, col_q)], out_w.at[sp, q, pl.ds(0, pool_ch)])
-        load(out_attn_w.at[:, pl.ds(q * col_q, col_q)], out_w.at[sp, q, pl.ds(pool_ch, q_width)])
+    quarters = SUBS if wide else 1
+    col_w = cols_dev // quarters
+    for q in range(quarters):
+        load(out_pool_w.at[:, pl.ds(q * col_w, col_w)], out_w.at[sp, q, pl.ds(0, pool_ch)])
+        load(out_attn_w.at[:, pl.ds(q * col_w, col_w)], out_w.at[sp, q, pl.ds(pool_ch, q_width)])
+    for src, dst in zip(small_refs, (gain, pool_w, pool_scale, row_cos, row_sin, col_cos, col_sin, spread)):
+        load(src, dst)
 
     def in_sub(owner, u):
         return in_w.at[owner, pl.ds(u * (depth // SUBS), depth // SUBS)]
@@ -168,7 +175,9 @@
     out_rows = pool_ch + q_width
 
     def out_sub(owner, u):
-        return out_w.at[owner, u // nr, pl.ds((u % nr) * (out_rows // nr), out_rows // nr)]
+        if wide:
+            return out_w.at[owner, u]
+        return out_w.at[owner, 0, pl.ds(u * (out_rows // SUBS), out_rows // SUBS)]
 
     def ring_copy(sub, sems, d, s, u):
         owner = owner_at(place - (s - 1) if d == 0 else place + (s - 1))
@@ -252,16 +261,17 @@
         )
 
     pl.semaphore_wait(barrier, len(greeted))
-    for copy in loads[:in_loads]:
-        copy.wait()
-    ring_start(in_ring, range(SUBS))
-    loads[in_loads].wait()
+    for u in range(SUBS):
+        for copy in loads[u * in_loads : (u + 1) * in_loads]:
+            copy.wait()
+        ring_start(in_ring, (u,))
+    loads[SUBS * in_loads].wait()
     for j in range(CHUNKS):
         for rel in range(1, chips):
             over_chips(rel, j, tp).start()
         over_cores(0, j, tp).start()
     acc[...] = jnp.zeros_like(acc)
-    for copy in loads[in_loads + 1 :]:
+    for copy in loads[SUBS * in_loads + 1 :]:
         copy.wait()
 
     @pl.when(sp == 0)
@@ -527,12 +537,17 @@
         own = m < nq
         return owner_at(place + jnp.where(own, 0, delta)), jnp.where(own, m, q)
 
-    def core_copy(m):
+    def weight_quarters(m, q):
+        final = m >= pieces - nq
+        return jnp.where(final, q, 2 * q), jnp.where(final, q + SUBS // 2, 2 * q + 1)
+
+    def core_copy(m, rel):
+        c = (chip + rel) % chips
         return pltpu.make_async_remote_copy(
-            src_ref=to_core.at[m],
-            dst_ref=from_core.at[m],
-            send_sem=core_send.at[m],
-            recv_sem=core_recv.at[m],
+            src_ref=to_core.at[m, c],
+            dst_ref=from_core.at[m, c],
+            send_sem=core_send.at[m, rel],
+            recv_sem=core_recv.at[m, rel],
             device_id=partner,
             device_id_type=MESH,
         )
@@ -549,22 +564,35 @@
 
     def multiply(m):
         owner, q = piece_at(m)
-        for mine, target in ((1 - core, to_core), (core, own_sum)):
-
-            def part(c, carry, mine=mine, target=target):
-                at = pl.ds(pl.multiple_of((2 * c + mine) * part_rows, part_rows), part_rows)
-                target[m, c] = jnp.dot(
-                    mixers[at, :], out_w[owner, q], preferred_element_type=jnp.float32
-                ).astype(jnp.bfloat16)
-                return carry
-
-            lax.fori_loop(0, chips, part, 0)
-            if target is to_core:
-                core_copy(m).start()
+
+        def part(k, carry):
+            rel = (k // 2 + 1) % chips
+            c = (chip + rel) % chips
+            mine = jnp.where(k % 2 == 0, 1 - core, core)
+            at = pl.ds(pl.multiple_of((2 * c + mine) * part_rows, part_rows), part_rows)
+            if wide:
+                first, second = weight_quarters(m, q)
+                weight = jnp.concatenate([out_w[owner, first], out_w[owner, second]], axis=1)
+            else:
+                weight = out_w[owner, q]
+            result = jnp.dot(mixers[at, :], weight, preferred_element_type=jnp.float32).astype(jnp.bfloat16)
+
+            @pl.when(k % 2 == 0)
+            def _():
+                to_core[m, c] = result
+                core_copy(m, rel).start()
+
+            @pl.when(k % 2 == 1)
+            def _():
+                own_sum[m, c] = result
+
+            return carry
+
+        lax.fori_loop(0, n_tp, part, 0)
 
     def pass_sum(m):
-        core_copy(m).wait_recv()
         for rel in range(1, chips):
+            core_copy(m, rel).wait_recv()
             c = (chip + rel) % chips
             both = own_sum[m, c].astype(jnp.float32) + from_core[m, c].astype(jnp.float32)
             own_sum[m, c] = both.astype(jnp.bfloat16)
@@ -572,18 +600,22 @@
 
     def total(m):
         owner, q = piece_at(m)
+        core_copy(m, 0).wait_recv()
         value = own_sum[m, chip].astype(jnp.float32) + from_core[m, chip].astype(jnp.float32)
         for rel in range(1, chips):
             chip_copy(m, rel).wait_recv()
             value = value + from_chip[m, rel - 1].astype(jnp.float32)
-        out[:, pl.ds(pl.multiple_of(owner * cols_dev + q * col_q, col_q), col_q)] = value.astype(out.dtype)
+        value = value.astype(out.dtype)
+        if wide:
+            for k, quarter in enumerate(weight_quarters(m, q)):
+                to = pl.ds(pl.multiple_of(owner * cols_dev + quarter * col_w, col_w), col_w)
+                out[:, to] = value[:, k * col_w : (k + 1) * col_w]
+        else:
+            out[:, pl.ds(pl.multiple_of(owner * cols_dev, cols_dev), cols_dev)] = value
 
     def piece(m, carry):
         multiply(m)
-
-        @pl.when(m > 0)
-        def _():
-            pass_sum(m - 1)
+        pass_sum(m)
 
         @pl.when(m >= LAG)
         def _():
@@ -608,8 +640,10 @@
     out_step(half - 1, True)
     for k in range(SUBS // 2):
         ring_last(ow_ring, k)
-    lax.fori_loop(pieces - nq, pieces, piece, 0)
-    pass_sum(pieces - 1)
+        if wide:
+            lax.fori_loop(pieces - nq + k, pieces - nq + k + 1, piece, 0)
+    if not wide:
+        lax.fori_loop(pieces - nq, pieces, piece, 0)
 
     def finish(m, carry):
         total(m)
@@ -631,8 +665,9 @@
             halo(k, False).wait_send()
 
     def sums_sent(m, carry):
-        core_copy(m).wait_send()
+        core_copy(m, 0).wait_send()
         for rel in range(1, chips):
+            core_copy(m, rel).wait_send()
             chip_copy(m, rel).wait_send()
         return carry
 
@@ -663,7 +698,8 @@
     out_rows = pool_ch + q_width
     half = n_sp // 2
     chips = n_tp // 2
-    nq = 2 if cols_dev >= 2 * LANES else 1
+    wide = cols_dev == SUBS * LANES
+    nq = SUBS // 2 if wide else 1
     col_q = cols_dev // nq
     pieces = n_sp * nq
     part_rows = rows // n_tp
@@ -673,11 +709,13 @@
         kv_parts = (key_weight, value_weight)
     tables = [jnp.asarray(t) for t in rotary_tables(rows * n_sp)]
     spread = jnp.asarray(spread_matrix(kvw), jnp.bfloat16)
-    dims = dict(sp=n_sp, tp=n_tp, kvw=kvw, nq=nq)
+    dims = dict(sp=n_sp, tp=n_tp, kvw=kvw, nq=nq, wide=wide)
+    small = (norm_gain.reshape(n_tp, 1, feats), pool_weight, pool_scale.reshape(1, pool_ch), *tables, spread)
     count = len(kv_parts)
 
     def kernel(*refs):
-        layer_kernel(dims, *refs[:3], refs[3 : 3 + count], *refs[3 + count :])
+        a, b = 3 + count, 5 + count
+        layer_kernel(dims, *refs[:3], refs[3:a], *refs[a:b], refs[b : b + len(small)], *refs[b + len(small) :])
 
     anywhere = pl.BlockSpec(memory_space=pl.ANY)
     vmem = pl.BlockSpec(memory_space=pltpu.VMEM)
@@ -685,13 +723,13 @@
     bf16, f32, dma = jnp.bfloat16, jnp.float32, pltpu.SemaphoreType.DMA
     return pl.pallas_call(
         kernel,
-        out_shape=jax.ShapeDtypeStruct((rows // n_tp, cols_dev * n_sp), bf16),
-        in_specs=[anywhere] * (5 + count) + [vmem] * 3 + [smem] + [vmem] * 5,
+        out_shape=pltpu.VMEM((rows // n_tp, cols_dev * n_sp), bf16),
+        in_specs=[anywhere] * (5 + count + len(small)) + [smem],
         out_specs=vmem,
         scratch_shapes=[
             pltpu.VMEM((n_tp, rows, feats), bf16),
             pltpu.VMEM((n_sp, depth, in_cols), bf16),
-            pltpu.VMEM((n_sp, nq, out_rows, col_q), bf16),
+            pltpu.VMEM((n_sp, SUBS if wide else 1, out_rows, LANES if wide else cols_dev), bf16),
             pltpu.VMEM((rows, in_cols), f32),
             pltpu.VMEM((rows, q_width), bf16),
             pltpu.VMEM((rows + 2 * POOL_PAD, pool_ch), bf16),
@@ -702,7 +740,8 @@
             pltpu.VMEM((pieces, chips, part_rows, col_q), bf16),
             pltpu.VMEM((pieces, chips, part_rows, col_q), bf16),
             pltpu.VMEM((pieces, chips - 1, part_rows, col_q), bf16),
-            dma((2 + count + 1 + 2 * nq,)),
+            *[pltpu.VMEM(value.shape, value.dtype) for value in small],
+            dma((SUBS * (2 + count) + 1 + 2 * (SUBS if wide else 1) + len(small),)),
             dma((2, half, SUBS)),
             dma((2, half, SUBS)),
             dma((2, half, SUBS)),
@@ -713,13 +752,13 @@
             dma((chips, CHUNKS)),
             dma((2, 2)),
             dma((2, 2)),
-            dma((pieces,)),
-            dma((pieces,)),
+            dma((pieces, chips)),
+            dma((pieces, chips)),
             dma((pieces, chips - 1)),
             dma((pieces, chips - 1)),
         ],
         compiler_params=pltpu.CompilerParams(
-            collective_id=0, has_side_effects=True, vmem_limit_bytes=67043328
+            collective_id=0, has_side_effects=True, vmem_limit_bytes=61 * 2**20
         ),
         name="layer",
     )(
@@ -729,12 +768,8 @@
         *kv_parts,
         out_pool_weight,
         out_attn_weight,
-        norm_gain.reshape(n_tp, 1, feats),
-        pool_weight,
-        pool_scale.reshape(1, pool_ch),
+        *small,
         sink_logit,
-        *tables,
-        spread,
     )
 
 

time: 206 us -> 198 us (0.961)
  Pallas kernels: 202 us -> 196 us
    pallas_call x1, Pallas kernels: 202 us -> 196 us  [shards(): pl.pallas_call(kernel, out_shape=pltpu.VMEM((rows // n_tp, cols_dev * n_s...]
where the time goes in v2:
time: 198 us
  Pallas kernels  196 us (99%)
    pallas_call x1, Pallas kernels, shards(): pl.pallas_call(kernel, out_shape=pltpu.VMEM((rows // n_tp, cols_dev * n_s...  196 us

profile of v2, /device:TPU:4, one launch (start us, length us, event | category | flops | bytes accessed | tf_op | source)
XLA Modules:
  0.0 197.7 jit_solution(4849328673040995925)
XLA Ops:
  0.0 196.3 %layer.1 = bf16[256,4096]{1,0:T(8,128)(2,1)S(1)} custom-call(bf16[1024,1024]{1,0:T(8,128)(2,1)} %refs_0_.1, bf16[512,512]{1,0:T(8,128)(2,1)} %refs_1_.1, bf16[512,512]{1,0:T(8,128)(2,1)} %refs_2_.1, bf16[512,128]{1,0:T(8,128)(2,1)} %refs_3_.1, bf16[512,128]{1,0:T(8,128)(2,1)} %refs_4_.1, bf16[512,512]{1,0:T(8,128)(2,1)} %refs_5_.1, ...), custom_call_target="tpu_custom_call" | custom-call | tf_op jit(solution)/shard_map/layer/pallas_call | solution.py:724
  196.4 1.3 copy.18

commit v3 on v2

--- a/solution.py
+++ b/solution.py
@@ -43,15 +43,12 @@
     return tables
 
 
-def spread_matrix(kv_width):
-    heads = kv_width // HEAD_DIM
-    spread = np.zeros((2 * kv_width, 4 * heads * LANES), np.float32)
-    for kind in range(2):
-        for head in range(heads):
-            for half in range(2):
-                block = (kind * heads + head) * 2 + half
-                for d in range(HEAD_DIM):
-                    spread[kind * kv_width + head * HEAD_DIM + d, block * LANES + half * HEAD_DIM + d] = 1.0
+def spread_matrix(heads, width):
+    spread = np.zeros((width, 2 * heads * LANES), np.float32)
+    for head in range(heads):
+        for half in range(2):
+            for d in range(HEAD_DIM):
+                spread[head * HEAD_DIM + d, (head * 2 + half) * LANES + half * HEAD_DIM + d] = 1.0
     return spread
 
 
@@ -60,19 +57,26 @@
     tokens,
     pool_in_w,
     query_w,
-    kv_parts,
+    key_w,
+    value_w,
     out_pool_w,
     out_attn_w,
     small_refs,
     sink,
     out,
     tok,
-    in_w,
+    in_a,
+    in_b,
+    mate_a,
+    mate_b,
     out_w,
     acc,
     queries,
     pool_pad,
     kv,
+    stage_pool,
+    stage_q,
+    stage_kv,
     kvx,
     mixers,
     to_core,
@@ -88,6 +92,8 @@
     col_sin,
     spread,
     load_sem,
+    pw_send,
+    pw_recv,
     in_send,
     in_recv,
     ow_send,
@@ -96,6 +102,10 @@
     tx_recv,
     td_send,
     td_recv,
+    ty_send,
+    ty_recv,
+    swap_send,
+    swap_recv,
     halo_send,
     halo_recv,
     core_send,
@@ -108,7 +118,10 @@
     depth = pool_in_w.shape[0]
     pool_ch = pool_in_w.shape[1]
     q_width = query_w.shape[1]
-    kvw = dims["kvw"]
+    heads_kv = dims["heads_kv"]
+    kv_width = key_w.shape[1]
+    pool_half = pool_ch // 2
+    q_half = q_width // 2
     cols_dev = out_pool_w.shape[1]
     nq = dims["nq"]
     wide = dims["wide"]
@@ -124,6 +137,13 @@
     chip = tp // 2
     core = tp % 2
     place = jnp.where(sp % 2 == 0, sp // 2, n_sp - 1 - sp // 2)
+    pairs = n_sp // 2
+    pair = sp // 2
+    member = sp % 2
+    mate = (pair * 2 + 1 - member, tp)
+
+    def pair_at(offset, which):
+        return (((pair + offset + pairs) % pairs) * 2 + which, tp)
 
     def owner_at(spot):
         spot = (spot + n_sp) % n_sp
@@ -140,7 +160,8 @@
         return ((chip - rel + chips) % chips) * 2 + core
 
     barrier = pltpu.get_barrier_semaphore()
-    greeted = [ahead, behind, ((sp + 1) % n_sp, tp), ((sp + n_sp - 1) % n_sp, tp), partner]
+    greeted = [ahead, behind, mate, partner]
+    greeted += [pair_at(offset, which) for offset in (1, -1) for which in (member, 1 - member)]
     greeted += [chip_peer(rel) for rel in range(1, chips)]
     for other in greeted:
         pl.semaphore_signal(barrier, inc=1, device_id=other, device_id_type=MESH)
@@ -148,19 +169,44 @@
     loads = []
 
     def load(src, dst):
-        copy = pltpu.make_async_copy(src, dst, load_sem.at[len(loads)])
+        copy = pltpu.make_async_copy(src, dst, load_sem.at[6 + len(loads)])
         copy.start()
         loads.append(copy)
 
-    sub_rows = depth // SUBS
-    for u in range(SUBS):
-        at = pl.ds(u * sub_rows, sub_rows)
-        start = 0
-        for part in (pool_in_w, query_w, *kv_parts):
-            load(part.at[at], in_w.at[sp, at, pl.ds(start, part.shape[1])])
-            start += part.shape[1]
-    in_loads = len(loads) // SUBS
-    load(tokens, tok.at[tp])
+    in_w = (in_a, in_b)
+
+    def local_loads(which, heads_to, pool_to, first):
+        parts = (
+            (query_w.at[:, pl.ds(which * q_half, q_half)], heads_to.at[:, pl.ds(0, q_half)]),
+            (key_w if which == 0 else value_w, heads_to.at[:, pl.ds(q_half, kv_width)]),
+            (pool_in_w.at[:, pl.ds(which * pool_half, pool_half)], pool_to),
+        )
+        return [pltpu.make_async_copy(src, dst, load_sem.at[first + k]) for k, (src, dst) in enumerate(parts)]
+
+    def own_load(which):
+        return local_loads(which, in_a.at[sp], in_b.at[sp], 0)
+
+    def mate_load(which):
+        return local_loads(which, mate_a, mate_b, 3)
+
+    def mate_weights(p):
+        return pltpu.make_async_remote_copy(
+            src_ref=(mate_a, mate_b)[p],
+            dst_ref=in_w[p].at[sp],
+            send_sem=pw_send.at[p],
+            recv_sem=pw_recv.at[p],
+            device_id=mate,
+            device_id_type=MESH,
+        )
+
+    for which in range(2):
+
+        @pl.when(member == which)
+        def _(which=which):
+            for copy in own_load(which) + mate_load(1 - which):
+                copy.start()
+
+    load(tokens, tok.at[member, tp])
     quarters = SUBS if wide else 1
     col_w = cols_dev // quarters
     for q in range(quarters):
@@ -169,8 +215,75 @@
     for src, dst in zip(small_refs, (gain, pool_w, pool_scale, row_cos, row_sin, col_cos, col_sin, spread)):
         load(src, dst)
 
-    def in_sub(owner, u):
-        return in_w.at[owner, pl.ds(u * (depth // SUBS), depth // SUBS)]
+    pass_cols = (pl.ds(pool_half, q_half + kv_width), pl.ds(0, pool_half))
+
+    def in_sub(p, which_pair, u):
+        owner = which_pair * 2 + (member if u == 0 else 1 - member)
+        return in_w[p].at[owner]
+
+    def line_exists(d, s):
+        return pair >= s if d == 0 else pair < pairs - s
+
+    def line_ref_copy(p, d, s, u, ref, target):
+        return pltpu.make_async_remote_copy(
+            src_ref=ref,
+            dst_ref=ref,
+            send_sem=in_send.at[p, d, s - 1, u],
+            recv_sem=in_recv.at[p, d, s - 1, u],
+            device_id=target,
+            device_id_type=MESH,
+        )
+
+    def line_copy(p, d, s, u):
+        ref = in_sub(p, pair - (s - 1) if d == 0 else pair + (s - 1), u)
+        return line_ref_copy(p, d, s, u, ref, pair_at(1 if d == 0 else -1, member))
+
+    def line_sends(d, s):
+        onward = pair < pairs - 1 if d == 0 else pair > 0
+        return onward & line_exists(d, s - 1)
+
+    def line_start(p, u):
+        for d in range(2):
+
+            @pl.when(line_sends(d, 1))
+            def _(d=d):
+                line_copy(p, d, 1, u).start()
+
+    def line_step(p, s, u, last=False):
+        for d in range(2):
+
+            @pl.when(line_exists(d, s))
+            def _(d=d):
+                ref = in_sub(p, pair - s if d == 0 else pair + s, u)
+                line_ref_copy(p, d, s, u, ref, pair_at(-1 if d == 0 else 1, member)).wait_recv()
+
+            if not last:
+
+                @pl.when(line_sends(d, s + 1))
+                def _(d=d):
+                    line_copy(p, d, s + 1, u).start()
+
+    def line_middle(p):
+        def step(s, carry):
+            for u in range(2):
+                line_step(p, s, u)
+            return carry
+
+        lax.fori_loop(3, pairs - 1, step, 0)
+
+    def line_sent():
+        def step(s, carry):
+            for p in range(2):
+                for u in range(2):
+                    for d in range(2):
+
+                        @pl.when(line_sends(d, s))
+                        def _(p=p, d=d, u=u):
+                            line_copy(p, d, s, u).wait_send()
+
+            return carry
+
+        lax.fori_loop(1, pairs, step, 0)
 
     out_rows = pool_ch + q_width
 
@@ -203,7 +316,6 @@
             device_id_type=MESH,
         ).wait_recv()
 
-    in_ring = (in_sub, (in_send, in_recv))
     ow_ring = (out_sub, (ow_send, ow_recv))
 
     def ring_start(ring, subs):
@@ -237,212 +349,233 @@
 
     chunk = rows // CHUNKS
 
-    def tok_rows(slot, j):
-        return tok.at[slot, pl.ds(j * chunk, chunk)]
-
-    def over_chips(rel, j, slot):
+    def tok_set(other):
+        return 1 - member if other else member
+
+    def tok_rows(other, slot, j):
+        return tok.at[tok_set(other), slot, pl.ds(j * chunk, chunk)]
+
+    def tok_copy(other, slot, j, sems, at, target):
+        ref = tok_rows(other, slot, j)
         return pltpu.make_async_remote_copy(
-            src_ref=tok_rows(slot, j),
-            dst_ref=tok_rows(slot, j),
-            send_sem=tx_send.at[rel - 1, j],
-            recv_sem=tx_recv.at[rel - 1, j],
-            device_id=chip_peer(rel),
+            src_ref=ref,
+            dst_ref=ref,
+            send_sem=sems[0].at[at],
+            recv_sem=sems[1].at[at],
+            device_id=target,
             device_id_type=MESH,
         )
 
-    def over_cores(rel, j, slot):
-        return pltpu.make_async_remote_copy(
-            src_ref=tok_rows(slot, j),
-            dst_ref=tok_rows(slot, j),
-            send_sem=td_send.at[rel, j],
-            recv_sem=td_recv.at[rel, j],
-            device_id=partner,
-            device_id_type=MESH,
-        )
+    def over_chips(other, rel, j, slot):
+        return tok_copy(other, slot, j, (tx_send, tx_recv), (int(other), rel - 1, j), chip_peer(rel))
+
+    def over_cores(other, rel, j, slot):
+        return tok_copy(other, slot, j, (td_send, td_recv), (int(other), rel, j), partner)
+
+    def over_pair(j, other):
+        return tok_copy(other, tp, j, (ty_send, ty_recv), (j,), mate)
+
+    def spread_tokens(other, j):
+        for rel in range(1, chips):
+            over_chips(other, rel, j, tp).start()
+        over_cores(other, 0, j, tp).start()
 
     pl.semaphore_wait(barrier, len(greeted))
-    for u in range(SUBS):
-        for copy in loads[u * in_loads : (u + 1) * in_loads]:
-            copy.wait()
-        ring_start(in_ring, (u,))
-    loads[SUBS * in_loads].wait()
+    for which in range(2):
+
+        @pl.when(member == which)
+        def _(which=which):
+            for copy in own_load(which) + mate_load(1 - which):
+                copy.wait()
+
+    for p in range(2):
+        mate_weights(p).start()
+    line_start(0, 0)
+    loads[0].wait()
     for j in range(CHUNKS):
-        for rel in range(1, chips):
-            over_chips(rel, j, tp).start()
-        over_cores(0, j, tp).start()
+        spread_tokens(False, j)
+        over_pair(j, False).start()
     acc[...] = jnp.zeros_like(acc)
-    for copy in loads[SUBS * in_loads + 1 :]:
+    for copy in loads[1:]:
         copy.wait()
 
     @pl.when(sp == 0)
     def _():
-        kv[pl.ds(0, WINDOW)] = jnp.zeros((WINDOW, kv.shape[1]), kv.dtype)
-        pool_pad[pl.ds(0, POOL_PAD)] = jnp.zeros((POOL_PAD, pool_ch), pool_pad.dtype)
+        kv[:, pl.ds(0, WINDOW)] = jnp.zeros((2, WINDOW, kv_width), kv.dtype)
+        pool_pad[:, pl.ds(0, POOL_PAD)] = jnp.zeros((2, POOL_PAD, pool_half), pool_pad.dtype)
 
     @pl.when(sp == n_sp - 1)
     def _():
-        kv[pl.ds(WINDOW + rows, WINDOW)] = jnp.zeros((WINDOW, kv.shape[1]), kv.dtype)
-        pool_pad[pl.ds(POOL_PAD + rows, POOL_PAD)] = jnp.zeros((POOL_PAD, pool_ch), pool_pad.dtype)
-
-    def pass_tokens(j):
+        kv[:, pl.ds(WINDOW + rows, WINDOW)] = jnp.zeros((2, WINDOW, kv_width), kv.dtype)
+        pool_pad[:, pl.ds(POOL_PAD + rows, POOL_PAD)] = jnp.zeros((2, POOL_PAD, pool_half), pool_pad.dtype)
+
+    def take_mate(j):
+        over_pair(j, True).wait_recv()
+        spread_tokens(True, j)
+
+    def pass_tokens(other, j):
         for rel in range(1, chips):
-            over_chips(rel, j, source_slot(rel)).wait_recv()
-            over_cores(rel, j, source_slot(rel)).start()
+            over_chips(other, rel, j, source_slot(rel)).wait_recv()
+            over_cores(other, rel, j, source_slot(rel)).start()
 
     norm_rows = 32
 
-    def normalise(j):
+    def normalise(other, j):
         for rel in range(chips):
             slot = source_slot(rel)
-            over_cores(rel, j, (slot // 2) * 2 + 1 - core).wait_recv()
-            over_cores(rel, j, slot).wait_send()
+            over_cores(other, rel, j, (slot // 2) * 2 + 1 - core).wait_recv()
+            over_cores(other, rel, j, slot).wait_send()
             if rel:
-                over_chips(rel, j, tp).wait_send()
+                over_chips(other, rel, j, tp).wait_send()
+        if not other:
+            over_pair(j, False).wait_send()
+        which = tok_set(other)
 
         def tile(i, carry):
             at = pl.ds(pl.multiple_of(j * chunk + i * norm_rows, norm_rows), norm_rows)
             total = jnp.zeros((norm_rows, 1), jnp.float32)
             for slot in range(n_tp):
-                floats = tok[slot, at, :].astype(jnp.float32)
+                floats = tok[which, slot, at, :].astype(jnp.float32)
                 total = total + jnp.sum(floats * floats, axis=-1, keepdims=True)
             scale = lax.rsqrt(total / (feats * n_tp) + epsilon)
             for slot in range(n_tp):
-                floats = tok[slot, at, :].astype(jnp.float32)
-                tok[slot, at, :] = ((floats * scale) * gain[slot]).astype(jnp.bfloat16)
+                floats = tok[which, slot, at, :].astype(jnp.float32)
+                tok[which, slot, at, :] = ((floats * scale) * gain[slot]).astype(jnp.bfloat16)
             return carry
 
         lax.fori_loop(0, chunk // norm_rows, tile, 0)
 
-    mm_rows = min(rows, 512)
-
-    def block_owner(i):
-        return owner_at(place + jnp.where(i % 2 == 1, -((i + 1) // 2), i // 2))
-
-    def project(first, last):
+    def project(other, p, first_chunk, last_chunk, near=True, far=True):
+        which = tok_set(other)
+        deep = 2 * depth
+
         def step(k, carry):
-            i, tile = k // (rows // mm_rows), k % (rows // mm_rows)
-            owner = block_owner(i)
-            at = pl.ds(pl.multiple_of(tile * mm_rows, mm_rows), mm_rows)
-            offset = owner * depth
-            part = tok[offset // feats, at, pl.ds(pl.multiple_of(offset % feats, depth), depth)]
-            acc[at, :] += jnp.dot(part, in_w[owner], preferred_element_type=jnp.float32)
+            j, owner = first_chunk + k // pairs, k % pairs
+
+            def add():
+                at = pl.ds(pl.multiple_of(j * chunk, chunk), chunk)
+                offset = owner * deep
+                part = tok[which, offset // feats, at, pl.ds(pl.multiple_of(offset % feats, deep), deep)]
+                weight = in_w[p][pl.ds(owner * 2, 2)].reshape(deep, -1)
+                acc[which, at, pass_cols[p]] += jnp.dot(part, weight, preferred_element_type=jnp.float32)
+
+            if near and far:
+                add()
+            else:
+                distant = jnp.abs(owner - pair) == pairs - 1
+                pl.when(distant if far else jnp.logical_not(distant))(add)
             return carry
 
-        lax.fori_loop(first * (rows // mm_rows), last * (rows // mm_rows), step, 0)
-
-    ring_step(in_ring, 1, 0, False)
-    pass_tokens(0)
-    ring_step(in_ring, 1, 1, False)
-    normalise(0)
-    ring_step(in_ring, 1, 2, False)
-    pass_tokens(1)
-    ring_step(in_ring, 1, 3, False)
-    normalise(1)
-    pass_tokens(2)
-    ring_step(in_ring, 2, 0, half == 3)
-    normalise(2)
-    ring_step(in_ring, 2, 1, half == 3)
-    pass_tokens(3)
-    ring_step(in_ring, 2, 2, half == 3)
-    normalise(3)
-    project(0, 3)
-    ring_step(in_ring, 2, 3, half == 3)
-    project(3, 5)
-
-    def middle_in(s, carry):
-        for u in range(SUBS):
-            ring_step(in_ring, s, u, False)
-        project(2 * s - 1, 2 * s + 1)
-        return carry
-
-    if half > 4:
-        lax.fori_loop(3, half - 1, middle_in, 0)
-    if half > 3:
-        for u in range(SUBS):
-            ring_step(in_ring, half - 1, u, True)
-        ring_start(ow_ring, range(SUBS // 2))
-        project(n_sp - 3, n_sp - 1)
-    for k in range(SUBS // 2):
-        ring_last(in_ring, k)
-    project(n_sp - 1, n_sp)
+        lax.fori_loop(0, (last_chunk - first_chunk) * pairs, step, 0)
 
     lane = lax.broadcasted_iota(jnp.int32, (GRID_W, LANES), 1)
     take_next = (lane % (HEAD_DIM // 2)) < HEAD_DIM // 4
-    kv_cols = 2 * kvw
-
-    def turn(i, carry):
-        at = pl.ds(pl.multiple_of(i * GRID_W, GRID_W), GRID_W)
-        grid_row = sp * (rows // GRID_W) + i
-        cosine = row_cos[pl.ds(grid_row, 1), :] + col_cos[...]
-        sine = row_sin[pl.ds(grid_row, 1), :] + col_sin[...]
-        to = pl.ds(pl.multiple_of(POOL_PAD + i * GRID_W, POOL_PAD), GRID_W)
-        pool_pad[to, :] = acc[at, pl.ds(0, pool_ch)].astype(jnp.bfloat16)
-
-        def turned(start):
-            raw = acc[at, pl.ds(start, LANES)]
-            other = jnp.where(
-                take_next,
-                pltpu.roll(raw, LANES - HEAD_DIM // 4, 1),
-                pltpu.roll(raw, HEAD_DIM // 4, 1),
+
+    def turn(other, p, first_chunk, last_chunk):
+        which = tok_set(other)
+
+        def pool_tile(i, carry):
+            at = pl.ds(pl.multiple_of(i * GRID_W, GRID_W), GRID_W)
+            pool_in = acc[which, at, pl.ds(0, pool_half)].astype(jnp.bfloat16)
+            stage_pool[which, at, :] = pool_in
+            if not other:
+                to = pl.ds(pl.multiple_of(POOL_PAD + i * GRID_W, POOL_PAD), GRID_W)
+                pool_pad[member, to, :] = pool_in
+            return carry
+
+        def head_tile(i, carry):
+            at = pl.ds(pl.multiple_of(i * GRID_W, GRID_W), GRID_W)
+            grid_row = (pair * 2 + which) * (rows // GRID_W) + i
+            cosine = row_cos[pl.ds(grid_row, 1), :] + col_cos[...]
+            sine = row_sin[pl.ds(grid_row, 1), :] + col_sin[...]
+
+            def turned(start):
+                raw = acc[which, at, pl.ds(start, LANES)]
+                moved = jnp.where(
+                    take_next,
+                    pltpu.roll(raw, LANES - HEAD_DIM // 4, 1),
+                    pltpu.roll(raw, HEAD_DIM // 4, 1),
+                )
+                return raw, raw * cosine + moved * sine
+
+            for slab in range(q_half // LANES):
+                _, values = turned(pool_half + slab * LANES)
+                values = (values * HEAD_DIM ** (-0.5)).astype(jnp.bfloat16)
+                if other:
+                    stage_q[at, pl.ds(slab * LANES, LANES)] = values
+                else:
+                    queries[member, at, pl.ds(slab * LANES, LANES)] = values
+            raw, values = turned(pool_half + q_half)
+            values = jnp.where(member == 0, values, raw).astype(jnp.bfloat16)
+            stage_kv[which, at, :] = values
+            if not other:
+                to = pl.ds(pl.multiple_of(WINDOW + i * GRID_W, GRID_W), GRID_W)
+                kv[member, to, :] = values
+            return carry
+
+        per_chunk = chunk // GRID_W
+        lax.fori_loop(first_chunk * per_chunk, last_chunk * per_chunk, pool_tile if p else head_tile, 0)
+
+    def swap(p, j, kind):
+        at = pl.ds(j * chunk, chunk)
+        return [
+            pltpu.make_async_remote_copy(
+                src_ref=src,
+                dst_ref=dst,
+                send_sem=swap_send.at[k, j],
+                recv_sem=swap_recv.at[k, j],
+                device_id=mate,
+                device_id_type=MESH,
             )
-            return raw, raw * cosine + other * sine
-
-        for slab in range(q_width // LANES):
-            _, values = turned(pool_ch + slab * LANES)
-            queries[at, pl.ds(slab * LANES, LANES)] = (values * HEAD_DIM ** (-0.5)).astype(jnp.bfloat16)
-        to = pl.ds(pl.multiple_of(WINDOW + i * GRID_W, GRID_W), GRID_W)
-        for slab in range(kv_cols // LANES):
-            begin = pool_ch + q_width + slab * LANES
-            turn_lanes = max(0, min(LANES, kvw - slab * LANES))
-            if turn_lanes == 0:
-                values = acc[at, pl.ds(begin, LANES)]
-            else:
-                raw, values = turned(begin)
-                if turn_lanes < LANES:
-                    values = jnp.where(lane < turn_lanes, values, raw)
-            kv[to, pl.ds(slab * LANES, LANES)] = values.astype(jnp.bfloat16)
-        return carry
-
-    lax.fori_loop(0, rows // GRID_W, turn, 0)
-
-    def halo(k, up):
-        ref, width = ((kv, WINDOW), (pool_pad, POOL_PAD))[k]
-        src = pl.ds(rows if up else width, width)
-        dst = pl.ds(0 if up else rows + width, width)
-        other = ((sp + 1) % n_sp if up else (sp + n_sp - 1) % n_sp, tp)
+            for k, (src, dst) in enumerate(
+                (
+                    (stage_kv.at[1 - member, at], kv.at[kind, pl.ds(WINDOW + j * chunk, chunk)]),
+                    (stage_q.at[at], queries.at[kind, at]),
+                    (stage_pool.at[1 - member, at], pool_pad.at[kind, pl.ds(POOL_PAD + j * chunk, chunk)]),
+                )
+            )
+            if (k == 2) == (p == 1)
+        ]
+
+    halo_parts = ((stage_kv, kv, WINDOW), (stage_pool, pool_pad, POOL_PAD))
+
+    def halo(k, kind, route):
+        stage, held, width = halo_parts[k]
+        top, low = pl.ds(rows - width, width), pl.ds(0, width)
+        if route == 0:
+            first = pl.ds(pl.multiple_of((1 - member) * (rows - width), width), width)
+            to = pl.ds(pl.multiple_of(member * (rows + width), width), width)
+            src, dst, target = stage.at[member, first], held.at[kind, to], mate
+        elif route == 1:
+            src, dst, target = stage.at[1, top], held.at[kind, low], pair_at(1, 0)
+        else:
+            src, dst, target = stage.at[0, low], held.at[kind, pl.ds(rows + width, width)], pair_at(-1, 1)
         return pltpu.make_async_remote_copy(
-            src_ref=ref.at[src],
-            dst_ref=ref.at[dst],
-            send_sem=halo_send.at[k, int(up)],
-            recv_sem=halo_recv.at[k, int(up)],
-            device_id=other,
+            src_ref=src,
+            dst_ref=dst,
+            send_sem=halo_send.at[k, kind, route],
+            recv_sem=halo_recv.at[k, kind, route],
+            device_id=target,
             device_id_type=MESH,
         )
 
-    @pl.when(sp < n_sp - 1)
-    def _():
-        for k in range(2):
-            halo(k, True).start()
-
-    @pl.when(sp > 0)
-    def _():
-        for k in range(2):
-            halo(k, False).start()
-
-    ring_start(ow_ring, range(SUBS // 2, SUBS))
+    def each_member(body):
+        for which in range(2):
+
+            @pl.when(member == which)
+            def _(which=which):
+                body(which)
+
+    kind_cols = 2 * heads_kv * LANES
 
     def spread_rows(start, count):
         at = pl.ds(start, count)
-        kvx[at, :] = jnp.dot(kv[at, :], spread[...], preferred_element_type=jnp.float32).astype(jnp.bfloat16)
-
-    def spread_tile(i, carry):
-        spread_rows(pl.multiple_of((i + 1) * WINDOW, WINDOW), WINDOW)
-        return carry
-
-    lax.fori_loop(0, rows // WINDOW, spread_tile, 0)
+        for kind in range(2):
+            kvx[at, pl.ds(kind * kind_cols, kind_cols)] = jnp.dot(
+                kv[kind, at, :], spread[...], preferred_element_type=jnp.float32
+            ).astype(jnp.bfloat16)
 
     span = 3 * WINDOW
-    heads_kv = kvw // HEAD_DIM
     group = Q_HEADS // KV_HEADS
     blocks = rows // WINDOW
 
@@ -457,10 +590,11 @@
         low = jnp.where((sp == 0) & (i == 0), WINDOW, 0)
         high = jnp.where((sp == n_sp - 1) & (i == blocks - 1), 2 * WINDOW, span)
         allowed = (key >= jnp.maximum(query, low)) & (key <= jnp.minimum(query + 2 * WINDOW, high - 1))
+        slabs_half = q_half // LANES
         for head in range(heads_kv):
-            for pair in range(group // 2):
-                slab = head * (group // 2) + pair
-                q_pair = queries[at, pl.ds(slab * LANES, LANES)]
+            for two in range(group // 2):
+                slab = head * (group // 2) + two
+                q_pair = queries[slab // slabs_half, at, pl.ds((slab % slabs_half) * LANES, LANES)]
                 result = jnp.zeros((WINDOW, LANES), jnp.float32)
                 for upper in range(2):
                     scores = lax.dot_general(
@@ -481,41 +615,163 @@
                 mixers[at, pl.ds(pool_ch + slab * LANES, LANES)] = result.astype(jnp.bfloat16)
         return carry
 
-    lax.fori_loop(1, blocks - 1, attend, 0)
+    per_chunk = chunk // WINDOW
+
+    def attend_chunk(j):
+        each_member(lambda which: [copy.wait_recv() for copy in swap(0, j, 1 - which)])
+        for b in range(per_chunk):
+            spread_rows(WINDOW + (j * per_chunk + b) * WINDOW, WINDOW)
+        lax.fori_loop(max(1, j * per_chunk - 1), (j + 1) * per_chunk - 1, attend, 0)
+
+    mate_weights(0).wait_recv()
+    line_start(0, 1)
+    line_step(0, 1, 0)
+    pass_tokens(False, 0)
+    line_step(0, 1, 1)
+    normalise(False, 0)
+    pass_tokens(False, 1)
+    take_mate(0)
+    line_step(0, 2, 0)
+    normalise(False, 1)
+    line_step(0, 2, 1)
+    line_middle(0)
+    mate_weights(1).wait_recv()
     for u in range(2):
-        ring_step(ow_ring, 1, u, False)
-
-    @pl.when(sp > 0)
+        line_start(1, u)
+    pass_tokens(False, 2)
+    take_mate(1)
+    normalise(False, 2)
+    line_step(0, pairs - 1, 0, True)
+    pass_tokens(False, 3)
+    take_mate(2)
+    line_step(0, pairs - 1, 1, True)
+    normalise(False, 3)
+
+    def mate_chunk(p, j, near=True):
+        project(True, p, j, j + 1, near=near)
+        turn(True, p, j, j + 1)
+        each_member(lambda which: [copy.start() for copy in swap(p, j, which)])
+
+    at_end = (pair == 0) | (pair == pairs - 1)
+
+    def early_ring(u):
+        @pl.when(at_end)
+        def _():
+            ring_start(ow_ring, (u,))
+
+    pass_tokens(True, 0)
+    line_step(1, 1, 0)
+    take_mate(3)
+    early_ring(0)
+    project(False, 0, 0, CHUNKS)
+    line_step(1, 1, 1)
+    early_ring(1)
+    normalise(True, 0)
+    mate_chunk(0, 0)
+    line_step(1, 2, 0)
+    pass_tokens(True, 1)
+    line_step(1, 2, 1)
+    line_middle(1)
+
+    @pl.when(jnp.logical_not(at_end))
     def _():
+        ring_start(ow_ring, range(SUBS))
+
+    early_ring(2)
+    normalise(True, 1)
+    mate_chunk(0, 1)
+    turn(False, 0, 0, CHUNKS)
+    early_ring(3)
+    project(False, 1, 0, CHUNKS, far=False)
+    pass_tokens(True, 2)
+    normalise(True, 2)
+    mate_chunk(0, 2)
+    project(True, 1, 0, CHUNKS - 1, far=False)
+    for j in range(CHUNKS - 2):
+        attend_chunk(j)
+    line_step(1, pairs - 1, 0, True)
+    line_step(1, pairs - 1, 1, True)
+    for j in range(CHUNKS - 1):
+        mate_chunk(1, j, near=False)
+    pass_tokens(True, CHUNKS - 1)
+    project(False, 1, 0, CHUNKS, near=False)
+    turn(False, 1, 0, CHUNKS)
+    normalise(True, CHUNKS - 1)
+    mate_chunk(0, CHUNKS - 1)
+    mate_chunk(1, CHUNKS - 1)
+
+    def halo_starts(which):
         for k in range(2):
-            halo(k, True).wait_recv()
-
-    @pl.when(sp < n_sp - 1)
+            halo(k, which, 0).start()
+
+        @pl.when(pair < pairs - 1)
+        def _():
+            for k in range(2):
+                halo(k, which, 1).start()
+
+        @pl.when(pair > 0)
+        def _():
+            for k in range(2):
+                halo(k, which, 2).start()
+
+    each_member(halo_starts)
+
+    @pl.when(member == 0)
     def _():
+        for stage, held, width in halo_parts:
+            held[0, pl.ds(rows + width, width)] = stage[1, pl.ds(0, width)]
+
+    @pl.when(member == 1)
+    def _():
+        for stage, held, width in halo_parts:
+            held[1, pl.ds(0, width)] = stage[0, pl.ds(rows - width, width)]
+
+    ring_step(ow_ring, 1, 0, False)
+    attend_chunk(CHUNKS - 2)
+    ring_step(ow_ring, 1, 1, False)
+    attend_chunk(CHUNKS - 1)
+    ring_step(ow_ring, 1, 2, False)
+
+    def halo_waits(which):
         for k in range(2):
-            halo(k, False).wait_recv()
-
+            halo(k, 1 - which, 0).wait_recv()
+
+        @pl.when(pair > 0 if which == 0 else pair < pairs - 1)
+        def _():
+            for k in range(2):
+                for kind in range(2):
+                    halo(k, kind, 1 if which == 0 else 2).wait_recv()
+
+    each_member(halo_waits)
     spread_rows(0, WINDOW)
     spread_rows(WINDOW + rows, WINDOW)
     lax.fori_loop(0, 2, lambda e, carry: attend(e * (blocks - 1), carry), 0)
-    ring_step(ow_ring, 1, 2, False)
+
+    each_member(lambda which: [copy.wait_recv() for j in range(CHUNKS) for copy in swap(1, j, 1 - which)])
 
     groups_dev = pool_ch // GROUP_DIM
     tile_rows = 256
 
     def pool_tile(i, carry):
         at = pl.ds(pl.multiple_of(i * tile_rows, tile_rows), tile_rows)
-        wide = tile_rows + 2 * POOL_PAD
-        row = lax.broadcasted_iota(jnp.int32, (tile_rows, wide), 0)
-        rel = lax.broadcasted_iota(jnp.int32, (tile_rows, wide), 1) - POOL_PAD - row
+        span_rows = tile_rows + 2 * POOL_PAD
+        row = lax.broadcasted_iota(jnp.int32, (tile_rows, span_rows), 0)
+        rel = lax.broadcasted_iota(jnp.int32, (tile_rows, span_rows), 1) - POOL_PAD - row
         position = sp * rows + i * tile_rows + lax.broadcasted_iota(jnp.int32, (tile_rows, LANES), 0)
         for g in range(groups_dev):
             level = (tp * groups_dev + g) % 4
             reach = jnp.where(level == 0, 1, jnp.where(level == 1, 2, jnp.where(level == 2, 4, 8)))
             band = jnp.where((rel >= -reach) & (rel < reach), 1.0, 0.0).astype(jnp.bfloat16)
             cols = pl.ds(g * GROUP_DIM, GROUP_DIM)
-            around = pool_pad[pl.ds(pl.multiple_of(i * tile_rows, tile_rows), wide), cols]
-            here = pool_pad[pl.ds(pl.multiple_of(i * tile_rows + POOL_PAD, POOL_PAD), tile_rows), cols]
+
+            def pool_rows(at_rows):
+                if pool_half >= GROUP_DIM:
+                    begin = g * GROUP_DIM
+                    return pool_pad[begin // pool_half, at_rows, pl.ds(begin % pool_half, GROUP_DIM)]
+                return jnp.concatenate([pool_pad[0, at_rows, :], pool_pad[1, at_rows, :]], axis=1)
+
+            around = pool_rows(pl.ds(pl.multiple_of(i * tile_rows, tile_rows), span_rows))
+            here = pool_rows(pl.ds(pl.multiple_of(i * tile_rows + POOL_PAD, POOL_PAD), tile_rows))
             window_sum = jnp.dot(band, around, preferred_element_type=jnp.float32)
             count = jnp.minimum(position + reach, n_sp * rows) - jnp.maximum(position - reach, 0)
             count = jnp.concatenate([count.astype(jnp.float32)] * (GROUP_DIM // LANES), axis=1)
@@ -651,18 +907,29 @@
 
     lax.fori_loop(pieces - LAG, pieces, finish, 0)
 
-    ring_sent(in_ring)
+    line_sent()
     ring_sent(ow_ring)
-
-    @pl.when(sp < n_sp - 1)
-    def _():
+    for p in range(2):
+        mate_weights(p).wait_send()
+
+    def pair_sent(which):
+        for j in range(CHUNKS):
+            for copy in swap(0, j, which) + swap(1, j, which):
+                copy.wait_send()
         for k in range(2):
-            halo(k, True).wait_send()
-
-    @pl.when(sp > 0)
-    def _():
-        for k in range(2):
-            halo(k, False).wait_send()
+            halo(k, which, 0).wait_send()
+
+        @pl.when(pair < pairs - 1)
+        def _():
+            for k in range(2):
+                halo(k, which, 1).wait_send()
+
+        @pl.when(pair > 0)
+        def _():
+            for k in range(2):
+                halo(k, which, 2).wait_send()
+
+    each_member(pair_sent)
 
     def sums_sent(m, carry):
         core_copy(m, 0).wait_send()
@@ -694,7 +961,7 @@
     q_width = query_weight.shape[1]
     kvw = key_weight.shape[1]
     cols_dev = out_pool_weight.shape[1]
-    in_cols = pool_ch + q_width + 2 * kvw
+    pool_half, q_half = pool_ch // 2, q_width // 2
     out_rows = pool_ch + q_width
     half = n_sp // 2
     chips = n_tp // 2
@@ -703,19 +970,17 @@
     col_q = cols_dev // nq
     pieces = n_sp * nq
     part_rows = rows // n_tp
-    if kvw % LANES:
-        kv_parts = (jnp.concatenate([key_weight, value_weight], axis=1),)
-    else:
-        kv_parts = (key_weight, value_weight)
+    kv_width = -(-kvw // LANES) * LANES
+    in_cols = pool_half + q_half + kv_width
+    if kv_width != kvw:
+        key_weight, value_weight = (jnp.pad(w, ((0, 0), (0, kv_width - kvw))) for w in (key_weight, value_weight))
     tables = [jnp.asarray(t) for t in rotary_tables(rows * n_sp)]
-    spread = jnp.asarray(spread_matrix(kvw), jnp.bfloat16)
-    dims = dict(sp=n_sp, tp=n_tp, kvw=kvw, nq=nq, wide=wide)
+    spread = jnp.asarray(spread_matrix(kvw // HEAD_DIM, kv_width), jnp.bfloat16)
+    dims = dict(sp=n_sp, tp=n_tp, heads_kv=kvw // HEAD_DIM, nq=nq, wide=wide)
     small = (norm_gain.reshape(n_tp, 1, feats), pool_weight, pool_scale.reshape(1, pool_ch), *tables, spread)
-    count = len(kv_parts)
 
     def kernel(*refs):
-        a, b = 3 + count, 5 + count
-        layer_kernel(dims, *refs[:3], refs[3:a], *refs[a:b], refs[b : b + len(small)], *refs[b + len(small) :])
+        layer_kernel(dims, *refs[:7], refs[7 : 7 + len(small)], *refs[7 + len(small) :])
 
     anywhere = pl.BlockSpec(memory_space=pl.ANY)
     vmem = pl.BlockSpec(memory_space=pltpu.VMEM)
@@ -724,16 +989,22 @@
     return pl.pallas_call(
         kernel,
         out_shape=pltpu.VMEM((rows // n_tp, cols_dev * n_sp), bf16),
-        in_specs=[anywhere] * (5 + count + len(small)) + [smem],
+        in_specs=[anywhere] * (7 + len(small)) + [smem],
         out_specs=vmem,
         scratch_shapes=[
-            pltpu.VMEM((n_tp, rows, feats), bf16),
-            pltpu.VMEM((n_sp, depth, in_cols), bf16),
+            pltpu.VMEM((2, n_tp, rows, feats), bf16),
+            pltpu.VMEM((n_sp, depth, q_half + kv_width), bf16),
+            pltpu.VMEM((n_sp, depth, pool_half), bf16),
+            pltpu.VMEM((depth, q_half + kv_width), bf16),
+            pltpu.VMEM((depth, pool_half), bf16),
             pltpu.VMEM((n_sp, SUBS if wide else 1, out_rows, LANES if wide else cols_dev), bf16),
-            pltpu.VMEM((rows, in_cols), f32),
-            pltpu.VMEM((rows, q_width), bf16),
-            pltpu.VMEM((rows + 2 * POOL_PAD, pool_ch), bf16),
-            pltpu.VMEM((rows + 2 * WINDOW, 2 * kvw), bf16),
+            pltpu.VMEM((2, rows, in_cols), f32),
+            pltpu.VMEM((2, rows, q_half), bf16),
+            pltpu.VMEM((2, rows + 2 * POOL_PAD, pool_half), bf16),
+            pltpu.VMEM((2, rows + 2 * WINDOW, kv_width), bf16),
+            pltpu.VMEM((2, rows, pool_half), bf16),
+            pltpu.VMEM((rows, q_half), bf16),
+            pltpu.VMEM((2, rows, kv_width), bf16),
             pltpu.VMEM((rows + 2 * WINDOW, 4 * (kvw // HEAD_DIM) * LANES), bf16),
             pltpu.VMEM((rows, out_rows), bf16),
             pltpu.VMEM((pieces, chips, part_rows, col_q), bf16),
@@ -741,17 +1012,23 @@
             pltpu.VMEM((pieces, chips, part_rows, col_q), bf16),
             pltpu.VMEM((pieces, chips - 1, part_rows, col_q), bf16),
             *[pltpu.VMEM(value.shape, value.dtype) for value in small],
-            dma((SUBS * (2 + count) + 1 + 2 * (SUBS if wide else 1) + len(small),)),
+            dma((7 + 2 * (SUBS if wide else 1) + len(small),)),
+            dma((2,)),
+            dma((2,)),
+            dma((2, 2, half, 2)),
+            dma((2, 2, half, 2)),
             dma((2, half, SUBS)),
             dma((2, half, SUBS)),
-            dma((2, half, SUBS)),
-            dma((2, half, SUBS)),
-            dma((chips - 1, CHUNKS)),
-            dma((chips - 1, CHUNKS)),
-            dma((chips, CHUNKS)),
-            dma((chips, CHUNKS)),
-            dma((2, 2)),
-            dma((2, 2)),
+            dma((2, chips - 1, CHUNKS)),
+            dma((2, chips - 1, CHUNKS)),
+            dma((2, chips, CHUNKS)),
+            dma((2, chips, CHUNKS)),
+            dma((CHUNKS,)),
+            dma((CHUNKS,)),
+            dma((3, CHUNKS)),
+            dma((3, CHUNKS)),
+            dma((2, 2, 3)),
+            dma((2, 2, 3)),
             dma((pieces, chips)),
             dma((pieces, chips)),
             dma((pieces, chips - 1)),
@@ -765,7 +1042,8 @@
         tokens,
         pool_in_weight,
         query_weight,
-        *kv_parts,
+        key_weight,
+        value_weight,
         out_pool_weight,
         out_attn_weight,
         *small,

time: 198 us -> 191 us (0.965)
  Pallas kernels: 196 us -> 188 us
    pallas_call x1, Pallas kernels: 196 us -> 188 us  [shards(): pl.pallas_call(kernel, out_shape=pltpu.VMEM((rows // n_tp, cols_dev * n_s...]
where the time goes in v3:
time: 191 us; the launch traced here: 189 us
  Pallas kernels  188 us (98%)
    pallas_call x1, Pallas kernels, shards(): pl.pallas_call(kernel, out_shape=pltpu.VMEM((rows // n_tp, cols_dev * n_s...  188 us

profile of v3, /device:TPU:4, one launch (start us, length us, event | category | flops | bytes accessed | tf_op | source)
XLA Modules:
  0.0 189.0 jit_solution(8457745938214791457)
XLA Ops:
  0.0 187.6 %layer.1 = bf16[256,4096]{1,0:T(8,128)(2,1)S(1)} custom-call(bf16[1024,1024]{1,0:T(8,128)(2,1)} %refs_0_.1, bf16[512,512]{1,0:T(8,128)(2,1)} %refs_1_.1, bf16[512,512]{1,0:T(8,128)(2,1)} %refs_2_.1, bf16[512,128]{1,0:T(8,128)(2,1)} %refs_3_.1, bf16[512,128]{1,0:T(8,128)(2,1)} %refs_4_.1, bf16[512,512]{1,0:T(8,128)(2,1)} %refs_5_.1, ...), custom_call_target="tpu_custom_call" | custom-call | tf_op jit(solution)/shard_map/layer/pallas_call | solution.py:989
  187.7 1.3 copy.18

commit v4 on v3

--- a/solution.py
+++ b/solution.py
@@ -448,12 +448,13 @@
     def project(other, p, first_chunk, last_chunk, near=True, far=True):
         which = tok_set(other)
         deep = 2 * depth
+        size = chunk * (2 if (last_chunk - first_chunk) % 2 == 0 else 1)
 
         def step(k, carry):
-            j, owner = first_chunk + k // pairs, k % pairs
+            j, owner = k // pairs, k % pairs
 
             def add():
-                at = pl.ds(pl.multiple_of(j * chunk, chunk), chunk)
+                at = pl.ds(pl.multiple_of(first_chunk * chunk + j * size, chunk), size)
                 offset = owner * deep
                 part = tok[which, offset // feats, at, pl.ds(pl.multiple_of(offset % feats, deep), deep)]
                 weight = in_w[p][pl.ds(owner * 2, 2)].reshape(deep, -1)
@@ -466,7 +467,7 @@
                 pl.when(distant if far else jnp.logical_not(distant))(add)
             return carry
 
-        lax.fori_loop(0, (last_chunk - first_chunk) * pairs, step, 0)
+        lax.fori_loop(0, (last_chunk - first_chunk) * chunk // size * pairs, step, 0)
 
     lane = lax.broadcasted_iota(jnp.int32, (GRID_W, LANES), 1)
     take_next = (lane % (HEAD_DIM // 2)) < HEAD_DIM // 4
@@ -623,6 +624,18 @@
             spread_rows(WINDOW + (j * per_chunk + b) * WINDOW, WINDOW)
         lax.fori_loop(max(1, j * per_chunk - 1), (j + 1) * per_chunk - 1, attend, 0)
 
+    def halo_starts(k, route):
+        def start(which):
+            def go():
+                halo(k, which, route).start()
+
+            if route == 0:
+                go()
+            else:
+                pl.when(pair < pairs - 1 if route == 1 else pair > 0)(go)
+
+        each_member(start)
+
     mate_weights(0).wait_recv()
     line_start(0, 1)
     line_step(0, 1, 0)
@@ -641,11 +654,14 @@
     pass_tokens(False, 2)
     take_mate(1)
     normalise(False, 2)
+    project(False, 0, 0, 2, far=False)
     line_step(0, pairs - 1, 0, True)
     pass_tokens(False, 3)
     take_mate(2)
+    project(False, 0, 2, 3, far=False)
     line_step(0, pairs - 1, 1, True)
     normalise(False, 3)
+    project(False, 0, 3, 4, far=False)
 
     def mate_chunk(p, j, near=True):
         project(True, p, j, j + 1, near=near)
@@ -659,11 +675,11 @@
         def _():
             ring_start(ow_ring, (u,))
 
+    early_ring(0)
     pass_tokens(True, 0)
     line_step(1, 1, 0)
     take_mate(3)
-    early_ring(0)
-    project(False, 0, 0, CHUNKS)
+    project(False, 0, 0, CHUNKS, near=False)
     line_step(1, 1, 1)
     early_ring(1)
     normalise(True, 0)
@@ -681,6 +697,8 @@
     normalise(True, 1)
     mate_chunk(0, 1)
     turn(False, 0, 0, CHUNKS)
+    halo_starts(0, 0)
+    halo_starts(0, 2)
     early_ring(3)
     project(False, 1, 0, CHUNKS, far=False)
     pass_tokens(True, 2)
@@ -696,25 +714,13 @@
     pass_tokens(True, CHUNKS - 1)
     project(False, 1, 0, CHUNKS, near=False)
     turn(False, 1, 0, CHUNKS)
+    halo_starts(1, 0)
+    halo_starts(1, 2)
     normalise(True, CHUNKS - 1)
     mate_chunk(0, CHUNKS - 1)
+    halo_starts(0, 1)
     mate_chunk(1, CHUNKS - 1)
-
-    def halo_starts(which):
-        for k in range(2):
-            halo(k, which, 0).start()
-
-        @pl.when(pair < pairs - 1)
-        def _():
-            for k in range(2):
-                halo(k, which, 1).start()
-
-        @pl.when(pair > 0)
-        def _():
-            for k in range(2):
-                halo(k, which, 2).start()
-
-    each_member(halo_starts)
+    halo_starts(1, 1)
 
     @pl.when(member == 0)
     def _():
@@ -726,8 +732,8 @@
         for stage, held, width in halo_parts:
             held[1, pl.ds(0, width)] = stage[0, pl.ds(rows - width, width)]
 
+    attend_chunk(CHUNKS - 2)
     ring_step(ow_ring, 1, 0, False)
-    attend_chunk(CHUNKS - 2)
     ring_step(ow_ring, 1, 1, False)
     attend_chunk(CHUNKS - 1)
     ring_step(ow_ring, 1, 2, False)

time: 191 us -> 189 us (0.990)
  Pallas kernels: 188 us -> 186 us
where the time goes in v4:
time: 189 us; the launch traced here: 188 us
  Pallas kernels  186 us (98%)
    pallas_call x1, Pallas kernels, shards(): pl.pallas_call(kernel, out_shape=pltpu.VMEM((rows // n_tp, cols_dev * n_s...  186 us

profile of v4, /device:TPU:4, one launch (start us, length us, event | category | flops | bytes accessed | tf_op | source)
XLA Modules:
  0.0 187.5 jit_solution(9758824877196585456)
XLA Ops:
  0.0 186.2 %layer.1 = bf16[256,4096]{1,0:T(8,128)(2,1)S(1)} custom-call(bf16[1024,1024]{1,0:T(8,128)(2,1)} %refs_0_.1, bf16[512,512]{1,0:T(8,128)(2,1)} %refs_1_.1, bf16[512,512]{1,0:T(8,128)(2,1)} %refs_2_.1, bf16[512,128]{1,0:T(8,128)(2,1)} %refs_3_.1, bf16[512,128]{1,0:T(8,128)(2,1)} %refs_4_.1, bf16[512,512]{1,0:T(8,128)(2,1)} %refs_5_.1, ...), custom_call_target="tpu_custom_call" | custom-call | tf_op jit(solution)/shard_map/layer/pallas_call | solution.py:995
  186.2 1.3 copy.18
